TPU v7x, 128 devices: a whole 4x4x4 slice. The times are simulated.
128 devices in a mesh: sp: 64 (over z, y, x), tp: 2 (over core).
Axes of the slice: x: 4, y: 4, z: 4, core: 2. Of those that a mesh axis runs over, the one named last changes fastest.
Arguments:
- tokens: bfloat16 [32768, 4096], P(('sp', 'tp')), may hold values from -6 to 6
- norm_gain: float32 [4096], replicated, may hold values from 0.5 to 1.5
- query_weight: bfloat16 [4096, 1024], P(None, 'tp'), may hold values from -0.09375 to 0.09375
- key_weight: bfloat16 [4096, 1024], P(None, 'tp'), may hold values from -0.09375 to 0.09375
- value_weight: bfloat16 [4096, 2048], P(None, 'tp'), may hold values from -0.09375 to 0.09375
- gate_weight: bfloat16 [4096, 2048], P(None, 'tp'), may hold values from -0.09375 to 0.09375
- decay_bias: float32 [1024], P('tp'), may hold values from -0.5 to 0.5
- head_gain: float32 [2048], P('tp'), may hold values from 0.5 to 1.5
- out_weight: bfloat16 [2048, 4096], P('tp'), may hold values from -0.125 to 0.125
Outputs:
- layer_out: bfloat16 [32768, 4096], P(('sp', 'tp'))
All inputs are finite; a program needn't handle non-finite values.
Results may differ from a plain program's by a relative error of at most 0.015.
Values may be sent and summed in bfloat16 or wider, within the bound.
A program may use at most 192 MiB of HBM per device.

v0:
```python
import math

import jax
import jax.numpy as jnp
from jax import lax
from jax.sharding import Mesh
from jax.sharding import PartitionSpec as P

HEAD_K = 128
HEAD_V = 256
BLOCK = 64
SP = ("sp_0", "sp_1", "sp_2")
SP_TP = ("sp_0", "sp_1", "sp_2", "tp")


epsilon = 1e-06
decay_power = 16.0
precise = lax.Precision.HIGHEST


def gathered_then(shard, axis, dim, work):
    return work(lax.all_gather(shard, axis, axis=dim, tiled=True), jnp.int32(0))


def filled_with(x, identity):
    return jax.tree.map(
        lambda a, e: jnp.broadcast_to(jnp.asarray(e, a.dtype), a.shape), x, identity
    )


def carried_in_2(x, axes, combine, identity, reverse):
    before = start = filled_with(x, identity)
    total = x
    for axis in reversed(axes):
        devices, position = lax.axis_size(axis), lax.axis_index(axis)
        pieces = jax.tree.map(lambda part: lax.all_gather(part, axis), total)
        inside, total = start, start
        for k in reversed(range(devices)) if reverse else range(devices):
            passed = k > position if reverse else k < position
            total = combine(total, jax.tree.map(lambda part: part[k], pieces))
            inside = jax.tree.map(lambda new, old: jnp.where(passed, new, old), total, inside)
        before = combine(inside, before)
    return before


def own_rows(portion, extent, axis):
    count = extent * lax.axis_size(axis)
    sent = portion(jnp.int32(0), count).astype(jnp.bfloat16)
    return lax.psum_scatter(sent, axis, scatter_dimension=0, tiled=True).astype(jnp.float32)


def to_blocks(values, head_width):
    block_count = values.shape[0] // BLOCK
    head_count = values.shape[1] // head_width
    return (
        values.astype(jnp.float32)
        .reshape(block_count, BLOCK, head_count, head_width)
        .transpose(2, 0, 1, 3)
    )


def combine(earlier_part, later_part):
    return (
        earlier_part[0] * later_part[0],
        later_part[0][..., None] * earlier_part[1] + later_part[1],
    )


def local_pass(queries, key_rows, value_rows, within, totals, start_state):
    block_end = totals[:, :, None, :]
    query_in = queries * jnp.exp(within)
    key_in = key_rows * jnp.exp(-within)
    key_out = key_rows * jnp.exp(block_end - within)
    causal = jnp.tril(jnp.ones((BLOCK, BLOCK), dtype=bool))
    scores = jnp.where(
        causal, jnp.einsum("hnid,hnjd->hnij", query_in, key_in, precision=precise), 0.0
    )
    local_out = jnp.einsum("hnij,hnjv->hniv", scores, value_rows, precision=precise)
    block_decay = jnp.exp(totals)

    def advance(carry_state, inputs_now):
        query_now, key_now, value_now, decay_now = inputs_now
        carried = jnp.einsum("hid,hdv->hiv", query_now, carry_state, precision=precise)
        carry_state = decay_now[..., None] * carry_state + jnp.einsum(
            "hjd,hjv->hdv", key_now, value_now, precision=precise
        )
        return (carry_state, carried)

    sequence_inputs = (
        jnp.moveaxis(query_in, 1, 0),
        jnp.moveaxis(key_out, 1, 0),
        jnp.moveaxis(value_rows, 1, 0),
        jnp.moveaxis(block_decay, 1, 0),
    )
    final_state, carried_out = lax.scan(advance, start_state, sequence_inputs)
    return (local_out + jnp.moveaxis(carried_out, 0, 1), final_state)


def mix_heads(queries, key_rows, value_rows, log_decay, carry):
    within = jnp.cumsum(log_decay, axis=2)
    totals = within[:, :, -1, :]
    before = jnp.cumsum(totals, axis=1) - totals
    span_end = before[:, -1, :] + totals[:, -1, :]
    through = within + before[:, :, None, :]
    key_out = key_rows * jnp.exp(span_end[:, None, None, :] - through)
    state_here = jnp.einsum("hncd,hncv->hdv", key_out, value_rows, precision=precise)
    carried_in = carry(jnp.exp(span_end), state_here)
    mixed_out, final_state = local_pass(queries, key_rows, value_rows, within, totals, carried_in)
    return mixed_out


def on_device(
    tokens,
    norm_gain,
    query_weight,
    key_weight,
    value_weight,
    gate_weight,
    decay_bias,
    head_gain,
    out_weight,
):
    inputs = tokens.astype(jnp.float32)
    row_scale = lax.rsqrt(jnp.mean(inputs * inputs, axis=-1, keepdims=True) + epsilon)
    normed = (inputs * row_scale * norm_gain.astype(jnp.float32)).astype(jnp.bfloat16)
    weights = (query_weight, key_weight, value_weight, gate_weight)

    def project(row_piece, row_start):
        return jnp.concatenate(
            [
                jnp.dot(row_piece, matrix, preferred_element_type=jnp.float32).astype(jnp.bfloat16)
                for matrix in weights
            ],
            axis=1,
        )

    projected = gathered_then(normed, "tp", 0, project)
    key_width = query_weight.shape[1]
    value_width = value_weight.shape[1]
    query_flat = projected[:, :key_width]
    key_flat = projected[:, key_width : 2 * key_width]
    value_flat = projected[:, 2 * key_width : 2 * key_width + value_width]
    gate_input = projected[:, 2 * key_width + value_width : 2 * key_width + 2 * value_width]
    span_rows = projected.shape[0]
    sequence = lax.axis_size(SP) * span_rows
    logits = decay_bias.astype(jnp.float32) + math.log(sequence / 8.0)
    log_decay = jnp.broadcast_to(jax.nn.log_sigmoid(logits) / decay_power, (span_rows, key_width))
    queries = to_blocks(query_flat, HEAD_K) * HEAD_K ** (-0.5)
    key_blocks = to_blocks(key_flat, HEAD_K)
    value_blocks = to_blocks(value_flat, HEAD_V)
    decay_blocks = to_blocks(log_decay, HEAD_K)
    head_count = queries.shape[0]

    def carry_all(span_decay, span_state):
        return carried_in_2(
            (span_decay, span_state),
            SP,
            combine,
            (jnp.ones_like(span_decay), jnp.zeros_like(span_state)),
            False,
        )[1]

    mixed_heads = mix_heads(queries, key_blocks, value_blocks, decay_blocks, carry_all)
    mixed_heads = mixed_heads.transpose(1, 2, 0, 3).reshape(span_rows, head_count, HEAD_V)
    head_scale = lax.rsqrt(jnp.mean(mixed_heads * mixed_heads, axis=-1, keepdims=True) + epsilon)
    normed_heads = (
        mixed_heads * head_scale * head_gain.astype(jnp.float32).reshape(head_count, HEAD_V)
    ).reshape(span_rows, head_count * HEAD_V)
    gated_rows = (normed_heads * jax.nn.silu(gate_input.astype(jnp.float32))).astype(jnp.bfloat16)
    rows_here = tokens.shape[0]

    def project_out(first_row, row_count):
        return jnp.dot(
            lax.dynamic_slice_in_dim(gated_rows, first_row, row_count, 0),
            out_weight,
            preferred_element_type=jnp.float32,
        )

    summed = own_rows(project_out, rows_here, "tp")
    return summed.astype(jnp.bfloat16)


def solution(mesh):
    finer = Mesh(mesh.devices.reshape(4, 4, 4, mesh.shape["tp"]), ("sp_0", "sp_1", "sp_2", "tp"))
    in_specs = (
        P(SP_TP, None),
        P(),
        P(None, "tp"),
        P(None, "tp"),
        P(None, "tp"),
        P(None, "tp"),
        P("tp"),
        P("tp"),
        P("tp", None),
    )
    out_specs = P(SP_TP, None)
    return jax.shard_map(
        on_device, mesh=finer, in_specs=in_specs, out_specs=out_specs, check_vma=False
    )
```

profile of v0, /device:TPU:32, one launch (start us, length us, event | category | flops | bytes accessed | tf_op | source)
XLA Modules:
  0.0 249.2 jit_solution(1708266083529635104)
XLA Ops:
  6.5 2.2 fusion.4
  8.8 2.7 %fusion.6 = bf16[256,4096]{1,0:T(8,128)(2,1)} fusion(bf16[256,4096]{1,0:T(8,128)(2,1)S(1)} %copy-done.3, f32[4096]{0:T(1024)} %param.12, f32[256]{0:T(256)S(1)} %add_rsqrt_fusion.1), kind=kLoop, calls=%fused_computation.14 | loop fusion | flops 4194304 | bytes 4211712 | tf_op jit(solution)/shard_map/convert_element_type | solution.py:125
  12.2 17.9 %all-gather.7.cloned.1.call-done = bf16[512,4096]{1,0:T(8,128)(2,1)} async-done(((bf16[256,4096]{1,0:T(8,128)(2,1)}), bf16[512,4096]{1,0:T(8,128)(2,1)}) %all-gather.7.cloned.1.call-update) | async-done | bytes 4194320 | tf_op jit(solution)/shard_map/all_gather | solution.py:22
  30.1 5.8 %fusion.12 = f32[512,512]{1,0:T(8,128)S(1)} fusion(bf16[512,4096]{1,0:T(8,128)(2,1)} %all-gather.7.cloned.1.call-done, bf16[4096,512]{1,0:T(8,128)(2,1)} %param.14), kind=kOutput, calls=%fused_computation.29 | convolution fusion | flops 2148007936 | bytes 9437184 | tf_op jit(solution)/shard_map/dot_general | solution.py:131
  36.3 5.8 %fusion.14 = f32[512,512]{1,0:T(8,128)S(1)} fusion(bf16[512,4096]{1,0:T(8,128)(2,1)} %all-gather.7.cloned.1.call-done, bf16[4096,512]{1,0:T(8,128)(2,1)} %param.13), kind=kOutput, calls=%fused_computation.32 | convolution fusion | flops 2148270080 | bytes 9437184 | tf_op jit(solution)/shard_map/dot_general | solution.py:131
  42.4 2.6 %bitcast_multiply_fusion.4 = (f32[4,8,64,128]{3,1,2,0:T(8,128)}, f32[4,8,64,128]{3,1,2,0:T(8,128)}, f32[4,8,64,128]{3,1,2,0:T(8,128)S(1)}) fusion(f32[8,64,4,128]{3,2,1,0:T(4,128)S(1)} %mul.334, f32[8,64,4,128]{3,2,1,0:T(4,128)S(1)} %reshape.176, f32[4,128]{1,0:T(4,128)S(1)} %fusion.47), kind=kOutput, calls=%fused_computation.44 | output fusion | flops 17301504 | bytes 5244928 | tf_op jit(solution)/shard_map/jit(cumsum)/reduce_window_sum | solution.py:100
  45.1 10.1 %convolution_convert_fusion.2 = bf16[512,1024]{1,0:T(8,128)(2,1)} fusion(bf16[512,4096]{1,0:T(8,128)(2,1)} %all-gather.7.cloned.1.call-done, bf16[4096,1024]{1,0:T(8,128)(2,1)} %param.15), kind=kOutput, calls=%fused_computation.26 | convolution fusion | flops 4295491584 | bytes 13631488 | tf_op jit(solution)/shard_map/dot_general | solution.py:131
  55.2 1.9 reshape.173
  57.1 3.4 %convolution_bitcast_fusion.1 = f32[4,128,256]{2,1,0:T(8,128)} fusion(bf16[8,64,4,256]{3,2,1,0:T(4,128)(2,1)S(1)} %reshape.173, f32[4,8,64,128]{3,1,2,0:T(8,128)S(1)} %get-tuple-element.103, f32[8,64,4,128]{3,2,1,0:T(4,128)S(1)} %reshape.176, f32[4,8,128]{2,1,0:T(8,128)S(1)} %get-tuple-element.89, f32[4,128]{1,0:T(4,128)S(1)} %bitcast.264), kind=kOutput, calls=%fused_computation.33 | convolution fusion | flops 806092800 | bytes 3688448 | tf_op jit(solution)/shard_map/hncd,hncv->hdv/dot_general | solution.py:106
  60.6 12.1 %all-gather = f32[16,1,128]{2,1,0:T(1,128)S(1)} all-gather(f32[4,1,128]{2,1,0:T(1,128)S(1)} %get-tuple-element.80), channel_id=2, replica_groups=mesh['sp_0'=4,'sp_1'=4,'sp_2'=4,'tp'=2] {'sp_2'}, dimensions={0}, use_global_device_ids=true | all-gather | bytes 10240 | tf_op jit(solution)/shard_map/all_gather | solution.py:36
  72.8 12.2 %all_gather.31 = f32[4,4,128]{2,1,0:T(4,128)S(1)} all-gather(f32[1,4,128]{2,1,0:T(4,128)S(1)} %get-tuple-element.100), channel_id=1, replica_groups=mesh['sp_0'=4,'sp_1'=4,'sp_2'=4,'tp'=2] {'sp_1'}, dimensions={0}, use_global_device_ids=true | all-gather | bytes 10240 | tf_op jit(solution)/shard_map/all_gather | solution.py:36
  84.9 7.7 %all-gather.13.cloned.1.call-done = f32[16,128,256]{2,1,0:T(8,128)} async-done(((f32[4,128,256]{2,1,0:T(8,128)}), f32[16,128,256]{2,1,0:T(8,128)}) %all-gather.13.cloned.1.call-update) | async-done | bytes 2097168 | tf_op jit(solution)/shard_map/all_gather | solution.py:36
  92.6 2.7 %bitcast_add_fusion.5 = f32[1,4,128,256]{3,2,1,0:T(8,128)} fusion(f32[16,128,256]{2,1,0:T(8,128)} %all-gather.13.cloned.1.call-done, f32[4,128]{1,0:T(4,128)S(1)} %get-tuple-element.98, f32[4,128]{1,0:T(4,128)S(1)} %get-tuple-element.102, f32[4,128]{1,0:T(4,128)S(1)} %bitcast.262, f32[4,128]{1,0:T(4,128)S(1)} %get-tuple-element.101), kind=kLoop, calls=%fused_computation.70 | loop fusion | flops 917504 | bytes 2629632 | tf_op jit(solution)/shard_map/add | solution.py:65
  95.5 30.6 %all-gather.9.cloned.1.call-done = f32[4,4,128,256]{3,2,1,0:T(8,128)} async-done(((f32[1,4,128,256]{3,2,1,0:T(8,128)}), f32[4,4,128,256]{3,2,1,0:T(8,128)}) %all-gather.9.cloned.1.call-update) | async-done | bytes 2097168 | tf_op jit(solution)/shard_map/all_gather | solution.py:36
  126.2 2.6 %multiply_add_fusion = f32[1,4,128,256]{3,2,1,0:T(8,128)} fusion(f32[4,4,128,256]{3,2,1,0:T(8,128)} %all-gather.9.cloned.1.call-done, f32[4,128]{1,0:T(4,128)S(1)} %get-tuple-element.99, f32[4,128]{1,0:T(4,128)S(1)} %get-tuple-element.97, f32[4,128]{1,0:T(4,128)S(1)} %get-tuple-element.96, f32[4,128]{1,0:T(4,128)S(1)} %get-tuple-element.95), kind=kLoop, calls=%fused_computation.77 | loop fusion | flops 917504 | bytes 2629632 | tf_op jit(solution)/shard_map/add | solution.py:65
  128.9 12.2 %all_gather.32 = f32[4,4,128]{2,1,0:T(4,128)S(1)} all-gather(f32[1,4,128]{2,1,0:T(4,128)S(1)} %get-tuple-element.94), channel_id=1, replica_groups=mesh['sp_0'=4,'sp_1'=4,'sp_2'=4,'tp'=2] {'sp_0'}, dimensions={0}, use_global_device_ids=true | all-gather | bytes 10240 | tf_op jit(solution)/shard_map/all_gather | solution.py:36
  142.8 3.0 %convolution_select_fusion = f32[4,8,64,64]{3,2,1,0:T(8,128)} fusion(f32[4,8,64,128]{3,1,2,0:T(8,128)S(1)} %copy-done.5, f32[4,8,64,128]{3,1,2,0:T(8,128)S(1)} %copy-done.4, pred[64,64]{1,0:T(8,128)(4,1)S(1)} %iota_compare_fusion), kind=kOutput, calls=%fused_computation.27 | convolution fusion | flops 201457664 | bytes 2625536 | tf_op jit(solution)/shard_map/hnid,hnjd->hnij/dot_general | solution.py:76
  145.8 2.6 %bitcast_multiply_fusion = (f32[8,4,64,128]{3,0,2,1:T(8,128)}, f32[8,4,64,128]{3,0,2,1:T(8,128)}) fusion(f32[4,8,64,128]{3,1,2,0:T(8,128)S(1)} %get-tuple-element.103, f32[8,64,4,128]{3,2,1,0:T(4,128)S(1)} %copy-done.1, f32[8,4,128]{2,0,1:T(8,128)S(1)} %get-tuple-element.88, f32[8,64,4,128]{3,2,1,0:T(4,128)S(1)} %reshape.176), kind=kLoop, calls=%fused_computation.34 | loop fusion | flops 786432 | bytes 5259264 | tf_op jit(solution)/shard_map/mul | solution.py:71
  148.4 10.3 %all-gather.11.cloned.1.call-done = f32[4,4,128,256]{3,2,1,0:T(8,128)} async-done(((f32[1,4,128,256]{3,2,1,0:T(8,128)}), f32[4,4,128,256]{3,2,1,0:T(8,128)}) %all-gather.11.cloned.1.call-update) | async-done | bytes 2097168 | tf_op jit(solution)/shard_map/all_gather | solution.py:36
  158.8 3.4 %fusion.30 = f32[4,128,256]{2,1,0:T(8,128)S(1)} fusion(f32[4,4,128,256]{3,2,1,0:T(8,128)} %all-gather.11.cloned.1.call-done, f32[4,4,128,256]{3,2,1,0:T(8,128)} %all-gather.9.cloned.1.call-done, f32[16,128,256]{2,1,0:T(8,128)} %all-gather.13.cloned.1.call-done, f32[4,128]{1,0:T(4,128)S(1)} %get-tuple-element.98, f32[4,128]{1,0:T(4,128)S(1)} %get-tuple-element.102, ...), kind=kLoop, calls=%fused_computation.56 | loop fusion | flops 4849664 | bytes 6844428 | tf_op jit(solution)/shard_map/add | solution.py:65
  162.2 36.9 %while.12 = (s32[]{:T(128)}, f32[4,128,256]{2,1,0:T(8,128)S(1)}, f32[8,4,64,256]{3,2,0,1:T(8,128)}, f32[8,4,128]{2,0,1:T(8,128)S(1)}, f32[8,4,64,128]{3,0,2,1:T(...) while((s32[]{:T(128)}, f32[4,128,256]{2,1,0:T(8,128)S(1)}, ...), condition=%wide.region_4.5_spmd, body=%wide.region_3.4_spmd.sunk | while | flops 201588736 | bytes 2890845 | solution.py:95
  162.2 1.8 constant_dynamic-slice_fusion.5
  166.9 1.7 constant_dynamic-slice_fusion.5
  171.5 1.7 constant_dynamic-slice_fusion.5
  176.1 1.7 constant_dynamic-slice_fusion.5
  180.7 1.7 constant_dynamic-slice_fusion.5
  185.3 1.7 constant_dynamic-slice_fusion.5
  199.1 4.1 %multiply_reduce_fusion = (f32[8,64,4]{1,0,2:T(8,128)S(1)}, f32[8,64,4,256]{3,1,0,2:T(8,128)}) fusion(f32[8,4,64,256]{3,2,0,1:T(8,128)} %get-tuple-element.42, f32[4,8,64,64]{3,2,1,0:T(8,128)S(1)} %copy-done.6, bf16[8,64,4,256]{3,2,1,0:T(4,128)(2,1)S(1)} %reshape.173), kind=kOutput, calls=%fused_computation.23 | convolution fusion | flops 404224000 | bytes 5775360 | tf_op jit(solution)/shard_map/hnij,hnjv->hniv/dot_general | solution.py:78
  204.0 1.8 copy.73
  207.3 1.8 copy.72
  209.2 17.5 %convolution_convert_fusion = bf16[512,4096]{1,0:T(8,128)(2,1)} fusion(bf16[1024,4096]{1,0:T(8,128)(2,1)} %param.19, f32[512,1024]{1,0:T(8,128)} %bitcast.255, f32[512,1024]{1,0:T(8,128)S(1)} %bitcast.254, bf16[512,4096]{1,0:T(8,128)(2,1)} %all-gather.7.cloned.1.call-done, bf16[4096,1024]{1,0:T(8,128)(2,1)} %param.16, f32[1024]{0:T(1024)S(1)} %copy-done.9), kind=kOutput, calls=%fused_computation.9 | convolution fusion | flops 8597274624 | bytes 29364224 | tf_op jit(solution)/shard_map/dot_general | solution.py:173
  226.6 16.1 %reduce-scatter.2.cloned.1.call-done = bf16[256,4096]{1,0:T(8,128)(2,1)} async-done(((bf16[512,4096]{1,0:T(8,128)(2,1)}), bf16[256,4096]{1,0:T(8,128)(2,1)}) %reduce-scatter.2.cloned.1.call-update) | async-done | bytes 2097168 | tf_op jit(solution)/shard_map/reduce_scatter | solution.py:49
  (77 shorter events, 32.0 us)
Async XLA Ops:
  6.5 2.2 copy-start.3
  6.5 23.6 %all-gather.7.cloned.1.call-start = ((), (), s32[]{:S(2)}) async-start(), calls=%async_computation.1 | async-start | bytes 6291456 | tf_op jit(solution)/shard_map/all_gather | solution.py:22
  11.5 0.7 copy-start.8
  11.5 81.1 %all-gather.13.cloned.1.call-start = ((), (), s32[]{:S(2)}) async-start(), calls=%async_computation.5 | async-start | bytes 2621440 | tf_op jit(solution)/shard_map/all_gather | solution.py:36
  42.4 2.6 %copy-start = (f32[8,64,4,128]{3,2,1,0:T(4,128)}, f32[8,64,4,128]{3,2,1,0:T(4,128)S(1)}, u32[]{:S(2)}) copy-start(f32[8,64,4,128]{3,2,1,0:T(4,128)S(1)} %mul.334) | copy-start | bytes 3145732
  60.6 65.6 %all-gather.9.cloned.1.call-start = ((), (), s32[]{:S(2)}) async-start(), calls=%async_computation.2 | async-start | bytes 2621440 | tf_op jit(solution)/shard_map/all_gather | solution.py:36
  95.3 63.5 %all-gather.11.cloned.1.call-start = ((), (), s32[]{:S(2)}) async-start(), calls=%async_computation.3 | async-start | bytes 2621440 | tf_op jit(solution)/shard_map/all_gather | solution.py:36
  128.8 113.9 %reduce-scatter.2.cloned.1.call-start = ((), (), s32[]{:S(2)}) async-start(), calls=%async_computation.4 | async-start | bytes 6291456 | tf_op jit(solution)/shard_map/reduce_scatter | solution.py:49
  128.9 13.9 %copy-start.4 = (f32[4,8,64,128]{3,1,2,0:T(8,128)S(1)}, f32[4,8,64,128]{3,1,2,0:T(8,128)}, u32[]{:S(2)}) copy-start(f32[4,8,64,128]{3,1,2,0:T(8,128)} %get-tuple-element.84) | copy-start | bytes 3145732
  128.9 13.9 %copy-start.5 = (f32[4,8,64,128]{3,1,2,0:T(8,128)S(1)}, f32[4,8,64,128]{3,1,2,0:T(8,128)}, u32[]{:S(2)}) copy-start(f32[4,8,64,128]{3,1,2,0:T(8,128)} %get-tuple-element.85) | copy-start | bytes 3145732
  142.8 3.0 %copy-start.1 = (f32[8,64,4,128]{3,2,1,0:T(4,128)S(1)}, f32[8,64,4,128]{3,2,1,0:T(4,128)}, u32[]{:S(2)}) copy-start(f32[8,64,4,128]{3,2,1,0:T(4,128)} %copy-done) | copy-start | bytes 3145732
  162.2 36.9 %copy-start.6 = (f32[4,8,64,64]{3,2,1,0:T(8,128)S(1)}, f32[4,8,64,64]{3,2,1,0:T(8,128)}, u32[]{:S(2)}) copy-start(f32[4,8,64,64]{3,2,1,0:T(8,128)} %convolution_select_fusion) | copy-start | bytes 1572868
  204.0 1.9 copy-start.2
  207.3 1.9 copy-start.7
  207.3 1.9 copy-start.9
Sparse Core Ops, SparseCore 0:
  11.6 18.4 all-gather.6
  60.7 31.8 all-gather.12
  95.4 30.7 all-gather.8
  128.9 29.7 all-gather.10
  226.8 15.8 reduce-scatter.1
where the time goes:
time: 251 us; the launch traced here: 249 us
  waiting for transfers between devices  82.7 us (33%)
  matrix products  72.2 us (29%)
  blocking collectives  36.5 us (15%)
  local copies, waits for them, and re-layouts  23.2 us (9%)
  other arithmetic  20.6 us (8%)
  between operations  13.4 us (5%)
    all_gather x3, waiting for transfers between devices, carried_in_2(): pieces = jax.tree.map(lambda part: lax.all_gather(part, axis), total)  48.7 us
    all_gather x3, blocking collectives, carried_in_2(): pieces = jax.tree.map(lambda part: lax.all_gather(part, axis), total)  36.5 us
    dot_general x3, matrix products, project(): jnp.dot(row_piece, matrix, preferred_element_type=jnp.float32)  21.7 us
    all_gather x1, waiting for transfers between devices, gathered_then(): return work(lax.all_gather(shard, axis, axis=dim, tiled=True), jnp.int32(0))  17.9 us
    dot_general x1, matrix products, project_out(): jnp.dot(lax.dynamic_slice_in_dim(gated_rows, first_row, row_count, 0), ou...  17.5 us
    reduce_scatter x1, waiting for transfers between devices, own_rows(): lax.psum_scatter(sent, axis, scatter_dimension=0, tiled=True)  16.1 us
    dynamic_slice x16, local copies, waits for them, and re-layouts, local_pass(): final_state, carried_out = lax.scan(advance, start_state, sequence_inputs)  14.1 us
    dot_general x8, matrix products, advance(): jnp.einsum('hjd,hjv->hdv', key_now, value_now, precision=precise)  13.5 us
  transfers between devices with their start and end apart: 5, of which 5 were waited for; matrix products, arithmetic and copies ran while one was open for 3% of the time, Pallas kernels for 0%

commit v1 on v0

v1 whole, which is shorter than its diff:
```python
import functools
import math

import jax
import jax.numpy as jnp
from jax import lax
from jax.experimental import pallas as pl
from jax.experimental.pallas import tpu as pltpu
from jax.sharding import Mesh
from jax.sharding import PartitionSpec as P

HEAD_K = 128
HEAD_V = 256
Z, Y, X, TP = "sp_0", "sp_1", "sp_2", "tp"
SP_TP = (Z, Y, X, TP)
MESH = pl.DeviceIdType.MESH
UNIT = 512
EPS = 1e-06
DECAY_POWER = 16.0
F32, BF16 = jnp.float32, jnp.bfloat16


def remote(src, dst, send, recv, where):
    return pltpu.make_async_remote_copy(
        src_ref=src, dst_ref=dst, send_sem=send, recv_sem=recv, device_id=where, device_id_type=MESH
    )


def dot(a, b, dims=((1,), (0,))):
    return lax.dot_general(a, b, (dims, ((), ())), preferred_element_type=F32)


def mixer(
    sizes,
    tok, gain, wq, wk, wv, wg, bias, hgain, wo,
    out,
    xn, wkb, wvb, wqb, wgb, wob, wpb, gainb, biasb, hgainb,
    kb, qb, vb, gsb, lob, sb, acc, ost,
    sa, ra, tb, rb, yp, tc, rc, dd, pd,
    gown, gsnd, grcv,
    tok_sem, w_sem, small_sem, wo_sem, out_sem,
    xs, xr, ps, pr, gs_s, gs_r, scan_s, scan_r,
):
    nz, ny, nx = sizes
    rows, width = xn.shape[1], xn.shape[2]
    heads = kb.shape[1]
    pairs = heads // 2
    chunk = HEAD_K // nx
    token_steps = tok_sem.shape[0]
    step_rows = rows // token_steps
    vsteps, osteps = wvb.shape[0], wob.shape[0]
    z, y, x, c = (lax.axis_index(a) for a in SP_TP)
    other = 1 - c
    chip = (z * ny + y) * nx + x
    seq = nz * ny * nx * 2 * rows

    def token_copy(i):
        r = pl.ds(i * step_rows, step_rows)
        return pltpu.make_async_copy(tok.at[r, :], xn.at[c, r, :], tok_sem.at[i])

    small = [(gain, gainb), (bias, biasb), (hgain, hgainb)]
    small = [pltpu.make_async_copy(a, b, small_sem.at[i]) for i, (a, b) in enumerate(small)]
    cols = lambda n: pl.ds(n * UNIT, UNIT)
    wk_copy = pltpu.make_async_copy(wk, wkb, w_sem.at[0])
    wq_copy = pltpu.make_async_copy(wq, wqb, w_sem.at[1])
    wv_copy = [pltpu.make_async_copy(wv.at[:, cols(n)], wvb.at[n], w_sem.at[2 + n]) for n in range(vsteps)]
    wg_copy = [pltpu.make_async_copy(wg.at[:, cols(n)], wgb.at[n], w_sem.at[2 + vsteps + n]) for n in range(vsteps)]
    wo_copy = [pltpu.make_async_copy(wo.at[:, cols(n)], wob.at[n], wo_sem.at[n]) for n in range(osteps)]
    for i in range(token_steps):
        token_copy(i).start()
    for s in small:
        s.start()
    for s in [wk_copy, *wv_copy, wq_copy, *wg_copy, *wo_copy]:
        s.start()

    barrier = pltpu.get_barrier_semaphore()
    peers = [{TP: other}]
    peers += [{X: lax.rem(x + d, nx)} for d in range(1, nx)]
    peers += [{Y: lax.rem(y + d, ny)} for d in range(1, ny)]
    peers += [{Z: lax.rem(z + d, nz)} for d in range(1, nz)]
    for peer in peers:
        pl.semaphore_signal(barrier, inc=1, device_id=peer, device_id_type=MESH)

    def x_send(i):
        r = pl.ds(i * step_rows, step_rows)
        return remote(xn.at[c, r, :], xn.at[c, r, :], xs.at[i], xr.at[i], {TP: other})

    def x_recv(i):
        r = pl.ds(i * step_rows, step_rows)
        return remote(xn.at[other, r, :], xn.at[other, r, :], xs.at[i], xr.at[i], {TP: other})

    for s in small:
        s.wait()
    for i in range(token_steps):
        token_copy(i).wait()

        @pl.loop(0, step_rows // 16)
        def _(g):
            r = pl.ds(pl.multiple_of(i * step_rows + g * 16, 16), 16)
            v = xn[c, r, :].astype(F32)
            scale = lax.rsqrt(jnp.mean(v * v, axis=-1, keepdims=True) + EPS)
            v = xn[c, r, :].astype(F32)
            xn[c, r, :] = (v * scale * gainb[...]).astype(BF16)

        if i == 0:
            pl.semaphore_wait(barrier, len(peers))
        x_send(i).start()

    logits = biasb[...] + math.log(seq / 8.0)
    log_decay = (jnp.minimum(logits, 0.0) - jnp.log1p(jnp.exp(-jnp.abs(logits)))) / DECAY_POWER

    def level(b):
        row = lax.broadcasted_iota(jnp.int32, (rows, 1), 0)
        pos = (row + (chip * 2 + b) * rows + (1 - seq // 2)).astype(F32)
        return pos * log_decay

    def scan_copy(phase, p, d, src, dst, axis, at, n):
        to = lax.rem(at + d, n)
        return remote(src, dst, scan_s.at[phase, p, d - 1], scan_r.at[phase, p, d - 1], {axis: to})

    def a_send(p, d):
        return scan_copy(0, p, d, sa.at[p, lax.rem(x + d, nx)], ra.at[p, x], X, x, nx)

    def a_recv(p, d):
        at = lax.rem(x + nx - d, nx)
        return scan_copy(0, p, d, sa.at[p, at], ra.at[p, at], X, x, nx)

    def b_send(p, d):
        return scan_copy(1, p, d, tb.at[p], rb.at[p, y], Y, y, ny)

    def b_recv(p, d):
        return scan_copy(1, p, d, tb.at[p], rb.at[p, lax.rem(y + ny - d, ny)], Y, y, ny)

    def c_send(p, d):
        return scan_copy(2, p, d, tc.at[p], rc.at[p, z], Z, z, nz)

    def c_recv(p, d):
        return scan_copy(2, p, d, tc.at[p], rc.at[p, lax.rem(z + nz - d, nz)], Z, z, nz)

    def d_send(p, d):
        return scan_copy(3, p, d, dd.at[p, lax.rem(x + d, nx)], pd.at[p, x], X, x, nx)

    def d_recv(p, d):
        at = lax.rem(x + nx - d, nx)
        return scan_copy(3, p, d, dd.at[p, at], pd.at[p, at], X, x, nx)

    def scan_a(p):
        for h in range(2):
            state = (sb[0, 2 * p + h] + sb[1, 2 * p + h]).astype(BF16)
            for i in range(nx):
                sa[p, i, h] = state[i * chunk : (i + 1) * chunk]
        for d in range(1, nx):
            a_send(p, d).start()
        ra[p, x] = sa[p, x]

    def scan_b(p):
        for d in range(1, nx):
            a_recv(p, d).wait_recv()
        total = ra[p, 0].astype(F32)
        for i in range(1, nx):
            total += ra[p, i].astype(F32)
        tb[p] = total.astype(BF16)
        for d in range(1, ny):
            b_send(p, d).start()
        rb[p, y] = tb[p]

    def scan_c(p):
        for d in range(1, ny):
            b_recv(p, d).wait_recv()
        total = jnp.zeros(tb.shape[1:], F32)
        before = jnp.zeros(tb.shape[1:], F32)
        for i in range(ny):
            part = rb[p, i].astype(F32)
            total += part
            before += jnp.where(i < y, part, 0.0)
        yp[p] = before
        tc[p] = total.astype(BF16)
        for d in range(1, nz):
            c_send(p, d).start()
        rc[p, z] = tc[p]

    def scan_d(p):
        for d in range(1, nz):
            c_recv(p, d).wait_recv()
        before = yp[p]
        for i in range(nz):
            before += jnp.where(i < z, rc[p, i].astype(F32), 0.0)
        for i in range(nx):
            dd[p, i] = before.astype(BF16)
            before += ra[p, i].astype(F32)
        for d in range(1, nx):
            d_send(p, d).start()
        pd[p, x] = dd[p, x]

    def scan_end(p):
        for d in range(1, nx):
            d_recv(p, d).wait_recv()

    @pl.loop(0, 2)
    def _(j):
        b = lax.rem(c + j, 2)

        @pl.when(j == 0)
        def _():
            wk_copy.wait()

        @pl.when(j == 1)
        def _():
            for i in range(token_steps):
                x_recv(i).wait_recv()

        keys = dot(xn[b], wkb[...]) * jnp.exp(-level(b))
        for h in range(heads):
            kb[b, h] = keys[:, h * HEAD_K : (h + 1) * HEAD_K].astype(BF16)
        for n in range(vsteps):

            @pl.when(j == 0)
            def _():
                wv_copy[n].wait()

            values = dot(xn[b], wvb[n]).astype(BF16)
            for i in range(2):
                h = 2 * n + i
                v = values[:, i * HEAD_V : (i + 1) * HEAD_V]
                vb[b, h] = v
                sb[b, h] = dot(kb[b, h], v, ((0,), (0,)))

            @pl.when(j == 1)
            def _():
                scan_a(n)

    wq_copy.wait()

    @pl.loop(0, 2)
    def _(b):
        queries = dot(xn[b], wqb[...]) * (jnp.exp(level(b)) * HEAD_K**-0.5)
        for h in range(heads):
            qb[b, h] = queries[:, h * HEAD_K : (h + 1) * HEAD_K].astype(BF16)

    def wo_send(n):
        return remote(wob.at[n], wpb.at[n], ps.at[n], pr.at[n], {TP: other})

    for n in range(osteps):
        wo_copy[n].wait()
        wo_send(n).start()

    for n in range(vsteps):
        wg_copy[n].wait()
    scan_b(0)

    @pl.loop(0, 2)
    def _(b):
        for n in range(vsteps):
            u = dot(xn[b], wgb[n])
            u = u / (1.0 + jnp.exp(-u)) * hgainb[:, n * UNIT : (n + 1) * UNIT]
            for i in range(2):
                gsb[b, 2 * n + i] = u[:, i * HEAD_V : (i + 1) * HEAD_V]

            if n == 0:

                @pl.when(b == 0)
                def _():
                    scan_b(1)

                @pl.when(b == 1)
                def _():
                    scan_c(0)

    scan_c(1)

    @pl.loop(0, heads)
    def _(h):
        for b in range(2):
            scores = dot(qb[b, h], kb[b, h], ((1,), (1,)))
            i = lax.broadcasted_iota(jnp.int32, scores.shape, 0)
            j = lax.broadcasted_iota(jnp.int32, scores.shape, 1)
            scores = jnp.where(i >= j, scores, 0.0).astype(BF16)
            lob[b, h] = dot(scores, vb[b, h])

    scan_d(0)
    scan_d(1)

    def g_send(h):
        p, i = divmod(h, 2)
        return remote(
            gsnd.at[p, i], grcv.at[p, i], gs_s.at[h], gs_r.at[h], {TP: other}
        )

    for p in range(pairs):
        scan_end(p)
        for i in range(2):
            h = 2 * p + i
            carried = pd[p, :, i].astype(F32).reshape(HEAD_K, HEAD_V)
            for own in range(2):
                b = c if own else other
                state = carried + jnp.where(b == 1, sb[0, h], 0.0)
                o = lob[b, h] + dot(qb[b, h], state.astype(BF16))
                scale = lax.rsqrt(jnp.mean(o * o, axis=-1, keepdims=True) + EPS)
                gated = (o * scale * gsb[b, h]).astype(BF16)
                if own:
                    gown[p, i] = gated
                else:
                    gsnd[p, i] = gated
                    g_send(h).start()
        if p == 0:
            for n in range(osteps):
                wo_send(n).wait_recv()
        for i in range(2):
            g_send(2 * p + i).wait_recv()

        @pl.loop(0, osteps)
        def _(n):
            part = acc[n] if p else None
            for i in range(2):
                r = slice((2 * p + i) * HEAD_V, (2 * p + i + 1) * HEAD_V)
                term = dot(gown[p, i], wob[n, r, :]) + dot(grcv[p, i], wpb[n, r, :])
                part = term if part is None else part + term
            if p < pairs - 1:
                acc[n] = part
            else:
                ost[n] = part.astype(BF16)

    for n in range(osteps):
        pltpu.make_async_copy(ost.at[n], out.at[:, cols(n)], out_sem.at[n]).start()
    for n in range(osteps):
        pltpu.make_async_copy(ost.at[n], out.at[:, cols(n)], out_sem.at[n]).wait()

    for i in range(token_steps):
        x_send(i).wait_send()
    for n in range(osteps):
        wo_send(n).wait_send()
    for h in range(heads):
        g_send(h).wait_send()
    for p in range(pairs):
        for d in range(1, nx):
            a_send(p, d).wait_send()
            d_send(p, d).wait_send()
        for d in range(1, ny):
            b_send(p, d).wait_send()
        for d in range(1, nz):
            c_send(p, d).wait_send()


def on_device(sizes, tok, gain, wq, wk, wv, wg, bias, hgain, wo):
    nz, ny, nx = sizes
    rows, width = tok.shape
    key_width, value_width, model = wq.shape[1], wv.shape[1], wo.shape[1]
    heads = key_width // HEAD_K
    pairs = heads // 2
    chunk = HEAD_K // nx
    vsteps, osteps = value_width // UNIT, model // UNIT
    token_steps = 4
    most = max(sizes) - 1
    vmem = pltpu.VMEM
    dma = pltpu.SemaphoreType.DMA
    quarter = (2, chunk, HEAD_V)
    scratch = [
        vmem((2, rows, width), BF16),
        vmem((width, key_width), BF16),
        vmem((vsteps, width, UNIT), BF16),
        vmem((width, key_width), BF16),
        vmem((vsteps, width, UNIT), BF16),
        vmem((osteps, value_width, UNIT), BF16),
        vmem((osteps, value_width, UNIT), BF16),
        vmem((1, width), F32),
        vmem((1, key_width), F32),
        vmem((1, value_width), F32),
        vmem((2, heads, rows, HEAD_K), BF16),
        vmem((2, heads, rows, HEAD_K), BF16),
        vmem((2, heads, rows, HEAD_V), BF16),
        vmem((2, heads, rows, HEAD_V), F32),
        vmem((2, heads, rows, HEAD_V), F32),
        vmem((2, heads, HEAD_K, HEAD_V), F32),
        vmem((osteps, rows, UNIT), F32),
        vmem((osteps, rows, UNIT), BF16),
        vmem((pairs, nx, *quarter), BF16),
        vmem((pairs, nx, *quarter), BF16),
        vmem((pairs, *quarter), BF16),
        vmem((pairs, ny, *quarter), BF16),
        vmem((pairs, *quarter), F32),
        vmem((pairs, *quarter), BF16),
        vmem((pairs, nz, *quarter), BF16),
        vmem((pairs, nx, *quarter), BF16),
        vmem((pairs, nx, *quarter), BF16),
        vmem((pairs, 2, rows, HEAD_V), BF16),
        vmem((pairs, 2, rows, HEAD_V), BF16),
        vmem((pairs, 2, rows, HEAD_V), BF16),
        dma((token_steps,)),
        dma((2 + 2 * vsteps,)),
        dma((3,)),
        dma((osteps,)),
        dma((osteps,)),
        dma((token_steps,)),
        dma((token_steps,)),
        dma((osteps,)),
        dma((osteps,)),
        dma((heads,)),
        dma((heads,)),
        dma((4, pairs, most)),
        dma((4, pairs, most)),
    ]
    hbm = pl.BlockSpec(memory_space=pl.ANY)
    return pl.pallas_call(
        functools.partial(mixer, sizes),
        out_shape=jax.ShapeDtypeStruct((rows, model), BF16),
        in_specs=[hbm] * 9,
        out_specs=hbm,
        scratch_shapes=scratch,
        compiler_params=pltpu.CompilerParams(
            collective_id=0, has_side_effects=True, vmem_limit_bytes=67_043_328
        ),
        name="mixer",
    )(
        tok, gain.reshape(1, -1), wq, wk, wv, wg, bias.reshape(1, -1), hgain.reshape(1, -1), wo
    )


def solution(mesh, sizes=(4, 4, 4)):
    finer = Mesh(mesh.devices.reshape(*sizes, mesh.shape["tp"]), SP_TP)
    in_specs = (
        P(SP_TP, None),
        P(),
        P(None, "tp"),
        P(None, "tp"),
        P(None, "tp"),
        P(None, "tp"),
        P("tp"),
        P("tp"),
        P("tp", None),
    )
    return jax.shard_map(
        functools.partial(on_device, sizes),
        mesh=finer,
        in_specs=in_specs,
        out_specs=P(SP_TP, None),
        check_vma=False,
    )
```

time: 251 us -> 56.9 us (0.23)
  the two profiles are of different devices: /device:TPU:32 before, /device:TPU:1 now
where the time goes in v1:
time: 56.9 us; the launch traced here: 56.8 us
  Pallas kernels  53.6 us (94%)
  local copies, waits for them, and re-layouts  3.13 us (6%)
    pallas_call x1, Pallas kernels, on_device(): pl.pallas_call(functools.partial(mixer, sizes), out_shape=jax.ShapeDtypeS...  53.6 us
    unnamed x1, local copies, waits for them, and re-layouts  3.13 us

profile of v1, /device:TPU:1, one launch (start us, length us, event | category | flops | bytes accessed | tf_op | source)
XLA Modules:
  0.0 56.8 jit_solution(4825290242042223447)
XLA Ops:
  0.0 53.6 %mixer.1 = bf16[256,4096]{1,0:T(8,128)(2,1)} custom-call(bf16[256,4096]{1,0:T(8,128)(2,1)} %tok.1, f32[1,4096]{1,0:T(1,128)} %bitcast.3, bf16[4096,512]{1,0:T(8,128)(2,1)} %wq.1, bf16[4096,512]{1,0:T(8,128)(2,1)} %wk.1, bf16[4096,1024]{1,0:T(8,128)(2,1)} %wv.1, bf16[4096,1024]{1,0:T(8,128)(2,1)} %wg.1, f32[1,512]{1,0:T(1,128)} %bitcast.5, ...), custom_call_target="tpu_custom_call" | custom-call | tf_op jit(solution)/shard_map/mixer/pallas_call | solution.py:403
  53.6 3.1 %copy.11 = bf16[256,4096]{1,0:T(8,128)(2,1)} copy(bf16[256,4096]{1,0:T(8,128)(2,1)} %mixer.1) | data formatting | bytes 4194304

commit v2 on v1

v2 whole, which is shorter than its diff:
```python
import functools
import math

import jax
import jax.numpy as jnp
from jax import lax
from jax.experimental import pallas as pl
from jax.experimental.pallas import tpu as pltpu
from jax.sharding import Mesh
from jax.sharding import PartitionSpec as P

HEAD_K = 128
HEAD_V = 256
Z, Y, X, TP = "sp_0", "sp_1", "sp_2", "tp"
SP_TP = (Z, Y, X, TP)
MESH = pl.DeviceIdType.MESH
UNIT = 512
EPS = 1e-06
DECAY_POWER = 16.0
F32, BF16 = jnp.float32, jnp.bfloat16


def remote(src, dst, send, recv, where):
    return pltpu.make_async_remote_copy(
        src_ref=src, dst_ref=dst, send_sem=send, recv_sem=recv, device_id=where, device_id_type=MESH
    )


def dot(a, b, dims=((1,), (0,))):
    return lax.dot_general(a, b, (dims, ((), ())), preferred_element_type=F32)


def mixer(
    sizes,
    tok, gain, wq, wk, wv, wg, bias, hgain, wo,
    out,
    xn, wkb, wvb, wqb, wgb, wob, gainb, biasb, hgainb,
    kb, qb, vb, gsb, lob, acc,
    sa, ra, tb, rb, yp, tc, rc, dd, pd,
    gall, gsnd,
    tok_sem, small_sem, k_sem, v_sem, q_sem, g_sem, wo_sem,
    xs, xr, ps, pr, gs_s, gs_r, scan_s, scan_r,
):
    nz, ny, nx = sizes
    rows, width = xn.shape[1], xn.shape[2]
    heads = kb.shape[1]
    pairs = heads // 2
    chunk = HEAD_K // nx
    token_steps = tok_sem.shape[0]
    step_rows = rows // token_steps
    model = out.shape[1]
    z, y, x, c = (lax.axis_index(a) for a in SP_TP)
    other = 1 - c
    chip = (z * ny + y) * nx + x
    seq = nz * ny * nx * 2 * rows

    def token_copy(i):
        r = pl.ds(i * step_rows, step_rows)
        return pltpu.make_async_copy(tok.at[r, :], xn.at[c, r, :], tok_sem.at[i])

    small = [(gain, gainb), (bias, biasb), (hgain, hgainb)]
    small = [pltpu.make_async_copy(a, b, small_sem.at[i]) for i, (a, b) in enumerate(small)]
    v2 = 2 * HEAD_V
    wk_copy = pltpu.make_async_copy(wk, wkb, k_sem.at[0])
    wv_copy = [pltpu.make_async_copy(wv.at[:, pl.ds(p * v2, v2)], wvb.at[p], v_sem.at[p]) for p in range(pairs)]
    wq_copy = pltpu.make_async_copy(wq, wqb, q_sem.at[0])
    wg_copy = [pltpu.make_async_copy(wg.at[:, pl.ds(p * v2, v2)], wgb.at[p], g_sem.at[p]) for p in range(pairs)]

    def wo_copy(h):
        return pltpu.make_async_copy(wo.at[pl.ds(h * HEAD_V, HEAD_V), :], wob.at[h, 0], wo_sem.at[h])

    def wo_send(h):
        return remote(wob.at[h, 0], wob.at[h, 1], ps.at[h], pr.at[h], {TP: other})

    for s in small:
        s.start()
    for i in range(token_steps):
        token_copy(i).start()
    wk_copy.start(priority=1)

    barrier = pltpu.get_barrier_semaphore()
    peers = [{TP: other}]
    peers += [{X: lax.rem(x + d, nx)} for d in range(1, nx)]
    peers += [{Y: lax.rem(y + d, ny)} for d in range(1, ny)]
    peers += [{Z: lax.rem(z + d, nz)} for d in range(1, nz)]
    for peer in peers:
        pl.semaphore_signal(barrier, inc=1, device_id=peer, device_id_type=MESH)

    def x_send(i):
        r = pl.ds(i * step_rows, step_rows)
        return remote(xn.at[c, r, :], xn.at[c, r, :], xs.at[i], xr.at[i], {TP: other})

    def x_recv(i):
        r = pl.ds(i * step_rows, step_rows)
        return remote(xn.at[other, r, :], xn.at[other, r, :], xs.at[i], xr.at[i], {TP: other})

    for s in small:
        s.wait()
    for i in range(token_steps):
        token_copy(i).wait()
        if i == token_steps - 1:
            for s in wv_copy:
                s.start(priority=1)

        for g in range(step_rows // 16):
            r = pl.ds(i * step_rows + g * 16, 16)
            v = xn[c, r, :].astype(F32)
            scale = lax.rsqrt(jnp.mean(v * v, axis=-1, keepdims=True) + EPS)
            v = xn[c, r, :].astype(F32)
            xn[c, r, :] = (v * scale * gainb[...]).astype(BF16)

        if i == 0:
            pl.semaphore_wait(barrier, len(peers))
        x_send(i).start()

    logits = biasb[...] + math.log(seq / 8.0)
    log_decay = (jnp.minimum(logits, 0.0) - jnp.log1p(jnp.exp(-jnp.abs(logits)))) / DECAY_POWER

    def level(b):
        row = lax.broadcasted_iota(jnp.int32, (rows, 1), 0)
        pos = (row + (chip * 2 + b) * rows + (1 - seq // 2)).astype(F32)
        return pos * log_decay

    def scan_copy(phase, h, d, src, dst, axis, at, n):
        to = lax.rem(at + d, n)
        return remote(src, dst, scan_s.at[phase, h, d - 1], scan_r.at[phase, h, d - 1], {axis: to})

    def a_send(h, d):
        return scan_copy(0, h, d, sa.at[h, lax.rem(x + d, nx)], ra.at[h, x], X, x, nx)

    def a_recv(h, d):
        at = lax.rem(x + nx - d, nx)
        return scan_copy(0, h, d, sa.at[h, at], ra.at[h, at], X, x, nx)

    def b_send(h, d):
        return scan_copy(1, h, d, tb.at[h], rb.at[h, y], Y, y, ny)

    def b_recv(h, d):
        return scan_copy(1, h, d, tb.at[h], rb.at[h, lax.rem(y + ny - d, ny)], Y, y, ny)

    def c_send(h, d):
        return scan_copy(2, h, d, tc.at[h], rc.at[h, d - 1], Z, z, nz)

    def c_recv(h, d):
        return scan_copy(2, h, d, tc.at[h], rc.at[h, d - 1], Z, z, nz)

    def d_send(h, d):
        return scan_copy(3, h, d, dd.at[h, lax.rem(x + d, nx)], pd.at[h, x], X, x, nx)

    def d_recv(h, d):
        at = lax.rem(x + nx - d, nx)
        return scan_copy(3, h, d, dd.at[h, at], pd.at[h, at], X, x, nx)

    far_first = lambda n: [2, 1, 3] if n == 4 else list(range(1, n))

    def scan_a(h):
        k = kb[:, h].reshape(2 * rows, HEAD_K)
        v = vb[:, h].reshape(2 * rows, HEAD_V)
        sa[h] = dot(k, v, ((0,), (0,))).astype(BF16).reshape(nx, chunk, HEAD_V)
        for d in far_first(nx):
            a_send(h, d).start()
        ra[h, x] = sa[h, x]

    def scan_b(h):
        for d in range(1, nx):
            a_recv(h, d).wait_recv()
        total = ra[h, 0].astype(F32)
        for i in range(1, nx):
            total += ra[h, i].astype(F32)
        tb[h] = total.astype(BF16)
        for d in far_first(ny):
            b_send(h, d).start()
        rb[h, y] = tb[h]

    def scan_c(h):
        for d in range(1, ny):
            b_recv(h, d).wait_recv()
        total = jnp.zeros(tb.shape[1:], F32)
        before = jnp.zeros(tb.shape[1:], F32)
        for i in range(ny):
            part = rb[h, i].astype(F32)
            total += part
            before += jnp.where(i < y, part, 0.0)
        tc[h] = total.astype(BF16)
        for d in far_first(nz):

            @pl.when(z + d < nz)
            def _():
                c_send(h, d).start()

        yp[h] = before

    def scan_d(h):
        for d in range(1, nz):

            @pl.when(z >= d)
            def _():
                c_recv(h, d).wait_recv()
                yp[h] += rc[h, d - 1].astype(F32)

        before = yp[h]
        for i in range(nx):
            dd[h, i] = before.astype(BF16)
            before += ra[h, i].astype(F32)
        for d in far_first(nx):
            d_send(h, d).start()
        pd[h, x] = dd[h, x]

    def scan_end(h):
        for d in range(1, nx):
            d_recv(h, d).wait_recv()

    def keys(b):
        k = dot(xn[b], wkb[...]) * jnp.exp(-level(b))
        for h in range(heads):
            kb[b, h] = k[:, h * HEAD_K : (h + 1) * HEAD_K].astype(BF16)

    def values(b, p):
        v = dot(xn[b], wvb[p]).astype(BF16)
        for i in range(2):
            vb[b, 2 * p + i] = v[:, i * HEAD_V : (i + 1) * HEAD_V]

    wk_copy.wait()
    keys(c)
    for h in range(heads):
        wo_copy(h).start(priority=1)
    wv_copy[0].wait()
    values(c, 0)
    wv_copy[1].wait()
    wq_copy.start(priority=1)
    for s in wg_copy:
        s.start(priority=1)
    values(c, 1)
    for i in range(token_steps):
        x_recv(i).wait_recv()
    keys(other)
    values(other, 0)
    scan_a(0)
    scan_a(1)
    wo_copy(0).wait()
    wo_send(0).start()
    values(other, 1)
    scan_a(2)
    scan_a(3)

    def queries(b):
        q = dot(xn[b], wqb[...]) * (jnp.exp(level(b)) * HEAD_K**-0.5)
        for h in range(heads):
            qb[b, h] = q[:, h * HEAD_K : (h + 1) * HEAD_K].astype(BF16)

    def gates(b, p):
        u = dot(xn[b], wgb[p])
        u = u / (1.0 + jnp.exp(-u)) * hgainb[:, p * v2 : (p + 1) * v2]
        for i in range(2):
            gsb[b, 2 * p + i] = u[:, i * HEAD_V : (i + 1) * HEAD_V].astype(BF16)

    def local(h):
        i = lax.broadcasted_iota(jnp.int32, (rows, rows), 0)
        j = lax.broadcasted_iota(jnp.int32, (rows, rows), 1)
        for b in range(2):
            scores = dot(qb[b, h], kb[b, h], ((1,), (1,)))
            scores = jnp.where(i >= j, scores, 0.0).astype(BF16)
            o = dot(scores, vb[b, h])
            if b:
                scores = dot(qb[b, h], kb[0, h], ((1,), (1,))).astype(BF16)
                o += dot(scores, vb[0, h])
            lob[b, h] = o.astype(BF16)

    wq_copy.wait()
    queries(0)
    scan_b(0)
    wo_copy(1).wait()
    wo_send(1).start()
    queries(1)
    scan_b(1)
    for s in wg_copy:
        s.wait()
    gates(0, 0)
    scan_b(2)
    scan_b(3)
    scan_c(0)
    wo_copy(2).wait()
    wo_send(2).start()
    gates(1, 0)
    scan_c(1)
    gates(0, 1)
    scan_c(2)
    scan_c(3)
    local(0)
    local(1)
    scan_d(0)
    wo_copy(3).wait()
    wo_send(3).start()
    gates(1, 1)
    scan_d(1)
    local(2)
    local(3)
    scan_d(2)
    scan_d(3)

    def g_send(h):
        return remote(gsnd.at[h], gall.at[h, 1], gs_s.at[h], gs_r.at[h], {TP: other})

    def carried(h):
        start = pd[h].reshape(HEAD_K, HEAD_V)
        for own in (False, True):
            b = c if own else other
            o = lob[b, h].astype(F32) + dot(qb[b, h], start)
            scale = lax.rsqrt(jnp.mean(o * o, axis=-1, keepdims=True) + EPS)
            gated = (o * scale * gsb[b, h].astype(F32)).astype(BF16)
            if own:
                gall[h, 0] = gated
            else:
                gsnd[h] = gated
                g_send(h).start()

    def project(h):
        gated = jnp.concatenate([gall[h, 0], gall[h, 1]], axis=1)
        for n in range(model // UNIT):
            at = slice(n * UNIT, (n + 1) * UNIT)
            part = dot(gated, wob[h, :, :, at].reshape(2 * HEAD_V, UNIT))
            if h:
                part += acc[n]
            if h < heads - 1:
                acc[n] = part
            else:
                out[:, at] = part.astype(BF16)

    scan_end(0)
    carried(0)
    for h in range(1, heads + 1):
        if h < heads:
            scan_end(h)
        g_send(h - 1).wait_recv()
        wo_send(h - 1).wait_recv()
        if h < heads:
            carried(h)
        project(h - 1)

    for i in range(token_steps):
        x_send(i).wait_send()
    for h in range(heads):
        wo_send(h).wait_send()
        g_send(h).wait_send()
        for d in range(1, nx):
            a_send(h, d).wait_send()
            d_send(h, d).wait_send()
        for d in range(1, ny):
            b_send(h, d).wait_send()
        for d in range(1, nz):

            @pl.when(z + d < nz)
            def _():
                c_send(h, d).wait_send()


def on_device(sizes, tok, gain, wq, wk, wv, wg, bias, hgain, wo):
    nz, ny, nx = sizes
    rows, width = tok.shape
    key_width, value_width, model = wq.shape[1], wv.shape[1], wo.shape[1]
    heads = key_width // HEAD_K
    pairs = heads // 2
    token_steps = 4
    most = max(sizes) - 1
    vmem = pltpu.VMEM
    dma = pltpu.SemaphoreType.DMA
    quarter = (HEAD_K // nx, HEAD_V)
    scratch = [
        vmem((2, rows, width), BF16),
        vmem((width, key_width), BF16),
        vmem((pairs, width, 2 * HEAD_V), BF16),
        vmem((width, key_width), BF16),
        vmem((pairs, width, 2 * HEAD_V), BF16),
        vmem((heads, 2, HEAD_V, model), BF16),
        vmem((1, width), F32),
        vmem((1, key_width), F32),
        vmem((1, value_width), F32),
        vmem((2, heads, rows, HEAD_K), BF16),
        vmem((2, heads, rows, HEAD_K), BF16),
        vmem((2, heads, rows, HEAD_V), BF16),
        vmem((2, heads, rows, HEAD_V), BF16),
        vmem((2, heads, rows, HEAD_V), BF16),
        vmem((model // UNIT, rows, UNIT), F32),
        vmem((heads, nx, *quarter), BF16),
        vmem((heads, nx, *quarter), BF16),
        vmem((heads, *quarter), BF16),
        vmem((heads, ny, *quarter), BF16),
        vmem((heads, *quarter), F32),
        vmem((heads, *quarter), BF16),
        vmem((heads, nz - 1, *quarter), BF16),
        vmem((heads, nx, *quarter), BF16),
        vmem((heads, nx, *quarter), BF16),
        vmem((heads, 2, rows, HEAD_V), BF16),
        vmem((heads, rows, HEAD_V), BF16),
        dma((token_steps,)),
        dma((3,)),
        dma((1,)),
        dma((pairs,)),
        dma((1,)),
        dma((pairs,)),
        dma((heads,)),
        dma((token_steps,)),
        dma((token_steps,)),
        dma((heads,)),
        dma((heads,)),
        dma((heads,)),
        dma((heads,)),
        dma((4, heads, most)),
        dma((4, heads, most)),
    ]
    hbm = pl.BlockSpec(memory_space=pl.ANY)
    return pl.pallas_call(
        functools.partial(mixer, sizes),
        out_shape=pltpu.VMEM((rows, model), BF16),
        in_specs=[hbm] * 9,
        out_specs=pl.BlockSpec(memory_space=pltpu.VMEM),
        scratch_shapes=scratch,
        compiler_params=pltpu.CompilerParams(
            collective_id=0, has_side_effects=True, vmem_limit_bytes=64_500_000
        ),
        name="mixer",
    )(
        tok, gain.reshape(1, -1), wq, wk, wv, wg, bias.reshape(1, -1), hgain.reshape(1, -1), wo
    )


def solution(mesh, sizes=(4, 4, 4)):
    finer = Mesh(mesh.devices.reshape(*sizes, mesh.shape["tp"]), SP_TP)
    in_specs = (
        P(SP_TP, None),
        P(),
        P(None, "tp"),
        P(None, "tp"),
        P(None, "tp"),
        P(None, "tp"),
        P("tp"),
        P("tp"),
        P("tp", None),
    )
    return jax.shard_map(
        functools.partial(on_device, sizes),
        mesh=finer,
        in_specs=in_specs,
        out_specs=P(SP_TP, None),
        check_vma=False,
    )
```

time: 56.9 us -> 40 us (0.70)
  Pallas kernels: 53.6 us -> 38.5 us
  local copies, waits for them, and re-layouts: 3.13 us -> 1.32 us
    pallas_call x1, Pallas kernels: 53.6 us -> 38.5 us  [on_device(): pl.pallas_call(functools.partial(mixer, sizes), out_shape=pltpu.VMEM((row...]
    unnamed x1, local copies, waits for them, and re-layouts: 3.13 us -> 1.32 us
where the time goes in v2:
time: 40 us; the launch traced here: 39.9 us
  Pallas kernels  38.5 us (96%)
  local copies, waits for them, and re-layouts  1.32 us (3%)
    pallas_call x1, Pallas kernels, on_device(): pl.pallas_call(functools.partial(mixer, sizes), out_shape=pltpu.VMEM((row...  38.5 us
    unnamed x1, local copies, waits for them, and re-layouts  1.32 us

profile of v2, /device:TPU:1, one launch (start us, length us, event | category | flops | bytes accessed | tf_op | source)
XLA Modules:
  0.0 39.9 jit_solution(17229472357209941864)
XLA Ops:
  0.0 38.5 %mixer.1 = bf16[256,4096]{1,0:T(8,128)(2,1)S(1)} custom-call(bf16[256,4096]{1,0:T(8,128)(2,1)} %tok.1, f32[1,4096]{1,0:T(1,128)} %bitcast.3, bf16[4096,512]{1,0:T(8,128)(2,1)} %wq.1, bf16[4096,512]{1,0:T(8,128)(2,1)} %wk.1, bf16[4096,1024]{1,0:T(8,128)(2,1)} %wv.1, bf16[4096,1024]{1,0:T(8,128)(2,1)} %wg.1, f32[1,512]{1,0:T(1,128)} %bitcast.5, ...), custom_call_target="tpu_custom_call" | custom-call | tf_op jit(solution)/shard_map/mixer/pallas_call | solution.py:412
  38.5 1.3 %copy.11 = bf16[256,4096]{1,0:T(8,128)(2,1)} copy(bf16[256,4096]{1,0:T(8,128)(2,1)S(1)} %mixer.1) | data formatting | bytes 4194304

commit v3 on v2

--- a/solution.py
+++ b/solution.py
@@ -39,7 +39,7 @@
     sa, ra, tb, rb, yp, tc, rc, dd, pd,
     gall, gsnd,
     tok_sem, small_sem, k_sem, v_sem, q_sem, g_sem, wo_sem,
-    xs, xr, ps, pr, gs_s, gs_r, scan_s, scan_r,
+    xs, xr, ps, pr, gs_s, gs_r, scan_s, scan_r, zsem,
 ):
     nz, ny, nx = sizes
     rows, width = xn.shape[1], xn.shape[2]
@@ -82,9 +82,13 @@
     peers = [{TP: other}]
     peers += [{X: lax.rem(x + d, nx)} for d in range(1, nx)]
     peers += [{Y: lax.rem(y + d, ny)} for d in range(1, ny)]
-    peers += [{Z: lax.rem(z + d, nz)} for d in range(1, nz)]
     for peer in peers:
         pl.semaphore_signal(barrier, inc=1, device_id=peer, device_id_type=MESH)
+    for d in range(1, nz):
+
+        @pl.when(z + d < nz)
+        def _():
+            pl.semaphore_signal(barrier, inc=1, device_id={Z: lax.rem(z + d, nz)}, device_id_type=MESH)
 
     def x_send(i):
         r = pl.ds(i * step_rows, step_rows)
@@ -109,9 +113,16 @@
             v = xn[c, r, :].astype(F32)
             xn[c, r, :] = (v * scale * gainb[...]).astype(BF16)
 
-        if i == 0:
-            pl.semaphore_wait(barrier, len(peers))
+
+    pl.semaphore_wait(barrier, len(peers) + z)
+    for i in range(token_steps):
         x_send(i).start()
+    for d in range(1, nz):
+
+        @pl.when(z >= d)
+        def _():
+            pl.semaphore_signal(zsem, inc=1, device_id={Z: lax.rem(z - d + nz, nz)}, device_id_type=MESH)
+
 
     logits = biasb[...] + math.log(seq / 8.0)
     log_decay = (jnp.minimum(logits, 0.0) - jnp.log1p(jnp.exp(-jnp.abs(logits)))) / DECAY_POWER
@@ -153,13 +164,16 @@
 
     far_first = lambda n: [2, 1, 3] if n == 4 else list(range(1, n))
 
-    def scan_a(h):
-        k = kb[:, h].reshape(2 * rows, HEAD_K)
-        v = vb[:, h].reshape(2 * rows, HEAD_V)
-        sa[h] = dot(k, v, ((0,), (0,))).astype(BF16).reshape(nx, chunk, HEAD_V)
-        for d in far_first(nx):
-            a_send(h, d).start()
-        ra[h, x] = sa[h, x]
+    def scan_a(pair):
+        for h in pair:
+            k = kb[:, h].reshape(2 * rows, HEAD_K)
+            v = vb[:, h].reshape(2 * rows, HEAD_V)
+            sa[h] = dot(k, v, ((0,), (0,))).astype(BF16).reshape(nx, chunk, HEAD_V)
+        for h in pair:
+            for d in far_first(nx):
+                a_send(h, d).start()
+        for h in pair:
+            ra[h, x] = sa[h, x]
 
     def scan_b(h):
         for d in range(1, nx):
@@ -190,7 +204,17 @@
 
         yp[h] = before
 
+        @pl.when(z == 0)
+        def _():
+            scan_back(h)
+
     def scan_d(h):
+        @pl.when(z > 0)
+        def _():
+            scan_z(h)
+            scan_back(h)
+
+    def scan_z(h):
         for d in range(1, nz):
 
             @pl.when(z >= d)
@@ -198,6 +222,7 @@
                 c_recv(h, d).wait_recv()
                 yp[h] += rc[h, d - 1].astype(F32)
 
+    def scan_back(h):
         before = yp[h]
         for i in range(nx):
             dd[h, i] = before.astype(BF16)
@@ -235,13 +260,11 @@
         x_recv(i).wait_recv()
     keys(other)
     values(other, 0)
-    scan_a(0)
-    scan_a(1)
+    scan_a((0, 1))
     wo_copy(0).wait()
     wo_send(0).start()
     values(other, 1)
-    scan_a(2)
-    scan_a(3)
+    scan_a((2, 3))
 
     def queries(b):
         q = dot(xn[b], wqb[...]) * (jnp.exp(level(b)) * HEAD_K**-0.5)
@@ -278,6 +301,11 @@
     gates(0, 0)
     scan_b(2)
     scan_b(3)
+
+    @pl.when(z + 1 < nz)
+    def _():
+        pl.semaphore_wait(zsem, nz - 1 - z)
+
     scan_c(0)
     wo_copy(2).wait()
     wo_send(2).start()
@@ -286,17 +314,17 @@
     gates(0, 1)
     scan_c(2)
     scan_c(3)
+    scan_d(0)
     local(0)
     local(1)
-    scan_d(0)
+    scan_d(1)
     wo_copy(3).wait()
     wo_send(3).start()
     gates(1, 1)
-    scan_d(1)
+    scan_d(2)
+    scan_d(3)
     local(2)
     local(3)
-    scan_d(2)
-    scan_d(3)
 
     def g_send(h):
         return remote(gsnd.at[h], gall.at[h, 1], gs_s.at[h], gs_r.at[h], {TP: other})
@@ -312,11 +340,10 @@
                 gall[h, 0] = gated
             else:
                 gsnd[h] = gated
-                g_send(h).start()
-
-    def project(h):
+
+    def project(h, steps):
         gated = jnp.concatenate([gall[h, 0], gall[h, 1]], axis=1)
-        for n in range(model // UNIT):
+        for n in steps:
             at = slice(n * UNIT, (n + 1) * UNIT)
             part = dot(gated, wob[h, :, :, at].reshape(2 * HEAD_V, UNIT))
             if h:
@@ -326,16 +353,29 @@
             else:
                 out[:, at] = part.astype(BF16)
 
+    first, rest = range(0, model // UNIT // 2), range(model // UNIT // 2, model // UNIT)
+
+    def arrived(h):
+        g_send(h).wait_recv()
+        wo_send(h).wait_recv()
+
     scan_end(0)
     carried(0)
-    for h in range(1, heads + 1):
-        if h < heads:
-            scan_end(h)
-        g_send(h - 1).wait_recv()
-        wo_send(h - 1).wait_recv()
-        if h < heads:
-            carried(h)
-        project(h - 1)
+    g_send(0).start()
+    scan_end(1)
+    carried(1)
+    g_send(1).start()
+    for h in range(2, heads):
+        scan_end(h)
+        arrived(h - 2)
+        carried(h)
+        project(h - 2, first)
+        g_send(h).start()
+        project(h - 2, rest)
+    for h in range(heads - 2, heads):
+        arrived(h)
+        project(h, first)
+        project(h, rest)
 
     for i in range(token_steps):
         x_send(i).wait_send()
@@ -407,6 +447,7 @@
         dma((heads,)),
         dma((4, heads, most)),
         dma((4, heads, most)),
+        pltpu.SemaphoreType.REGULAR,
     ]
     hbm = pl.BlockSpec(memory_space=pl.ANY)
     return pl.pallas_call(

time: 40 us -> 36.4 us (0.910)
  Pallas kernels: 38.5 us -> 34.9 us
    pallas_call x1, Pallas kernels: 38.5 us -> 34.9 us  [on_device(): pl.pallas_call(functools.partial(mixer, sizes), out_shape=pltpu.VMEM((row...]
where the time goes in v3:
time: 36.4 us; the launch traced here: 36.3 us
  Pallas kernels  34.9 us (96%)
  local copies, waits for them, and re-layouts  1.32 us (4%)
    pallas_call x1, Pallas kernels, on_device(): pl.pallas_call(functools.partial(mixer, sizes), out_shape=pltpu.VMEM((row...  34.9 us
    unnamed x1, local copies, waits for them, and re-layouts  1.32 us

profile of v3, /device:TPU:1, one launch (start us, length us, event | category | flops | bytes accessed | tf_op | source)
XLA Modules:
  0.0 36.3 jit_solution(9083739994006811359)
XLA Ops:
  0.0 34.9 %mixer.1 = bf16[256,4096]{1,0:T(8,128)(2,1)S(1)} custom-call(bf16[256,4096]{1,0:T(8,128)(2,1)} %tok.1, f32[1,4096]{1,0:T(1,128)} %bitcast.3, bf16[4096,512]{1,0:T(8,128)(2,1)} %wq.1, bf16[4096,512]{1,0:T(8,128)(2,1)} %wk.1, bf16[4096,1024]{1,0:T(8,128)(2,1)} %wv.1, bf16[4096,1024]{1,0:T(8,128)(2,1)} %wg.1, f32[1,512]{1,0:T(1,128)} %bitcast.5, ...), custom_call_target="tpu_custom_call" | custom-call | tf_op jit(solution)/shard_map/mixer/pallas_call | solution.py:453
  34.9 1.3 %copy.11 = bf16[256,4096]{1,0:T(8,128)(2,1)} copy(bf16[256,4096]{1,0:T(8,128)(2,1)S(1)} %mixer.1) | data formatting | bytes 4194304

commit v4 on v3

--- a/solution.py
+++ b/solution.py
@@ -39,7 +39,7 @@
     sa, ra, tb, rb, yp, tc, rc, dd, pd,
     gall, gsnd,
     tok_sem, small_sem, k_sem, v_sem, q_sem, g_sem, wo_sem,
-    xs, xr, ps, pr, gs_s, gs_r, scan_s, scan_r, zsem,
+    xs, xr, ps, pr, gs_s, gs_r, scan_s, scan_r, line_sem,
 ):
     nz, ny, nx = sizes
     rows, width = xn.shape[1], xn.shape[2]
@@ -79,16 +79,30 @@
     wk_copy.start(priority=1)
 
     barrier = pltpu.get_barrier_semaphore()
-    peers = [{TP: other}]
-    peers += [{X: lax.rem(x + d, nx)} for d in range(1, nx)]
-    peers += [{Y: lax.rem(y + d, ny)} for d in range(1, ny)]
-    for peer in peers:
-        pl.semaphore_signal(barrier, inc=1, device_id=peer, device_id_type=MESH)
-    for d in range(1, nz):
-
-        @pl.when(z + d < nz)
+    lines = [(X, x, nx), (Y, y, ny), (Z, z, nz)]
+    pl.semaphore_signal(barrier, inc=1, device_id={TP: other}, device_id_type=MESH)
+    for axis, at, n in lines:
+        for d in range(1, n):
+
+            @pl.when(at + d < n)
+            def _():
+                pl.semaphore_signal(barrier, inc=1, device_id={axis: lax.rem(at + d, n)}, device_id_type=MESH)
+
+    def tell_earlier():
+        for i, (axis, at, n) in enumerate(lines):
+            for d in range(1, n):
+
+                @pl.when(at >= d)
+                def _():
+                    to = {axis: lax.rem(at - d + n, n)}
+                    pl.semaphore_signal(line_sem.at[i], inc=1, device_id=to, device_id_type=MESH)
+
+    def later_are_in(i):
+        _, at, n = lines[i]
+
+        @pl.when(at + 1 < n)
         def _():
-            pl.semaphore_signal(barrier, inc=1, device_id={Z: lax.rem(z + d, nz)}, device_id_type=MESH)
+            pl.semaphore_wait(line_sem.at[i], n - 1 - at)
 
     def x_send(i):
         r = pl.ds(i * step_rows, step_rows)
@@ -102,9 +116,10 @@
         s.wait()
     for i in range(token_steps):
         token_copy(i).wait()
+        if i == 0:
+            wv_copy[0].start(priority=1)
         if i == token_steps - 1:
-            for s in wv_copy:
-                s.start(priority=1)
+            wv_copy[1].start(priority=1)
 
         for g in range(step_rows // 16):
             r = pl.ds(i * step_rows + g * 16, 16)
@@ -112,17 +127,12 @@
             scale = lax.rsqrt(jnp.mean(v * v, axis=-1, keepdims=True) + EPS)
             v = xn[c, r, :].astype(F32)
             xn[c, r, :] = (v * scale * gainb[...]).astype(BF16)
-
-
-    pl.semaphore_wait(barrier, len(peers) + z)
-    for i in range(token_steps):
+        if i == 0:
+            pl.semaphore_wait(barrier, 1 + x + y + z)
         x_send(i).start()
-    for d in range(1, nz):
-
-        @pl.when(z >= d)
-        def _():
-            pl.semaphore_signal(zsem, inc=1, device_id={Z: lax.rem(z - d + nz, nz)}, device_id_type=MESH)
-
+
+
+    tell_earlier()
 
     logits = biasb[...] + math.log(seq / 8.0)
     log_decay = (jnp.minimum(logits, 0.0) - jnp.log1p(jnp.exp(-jnp.abs(logits)))) / DECAY_POWER
@@ -144,10 +154,10 @@
         return scan_copy(0, h, d, sa.at[h, at], ra.at[h, at], X, x, nx)
 
     def b_send(h, d):
-        return scan_copy(1, h, d, tb.at[h], rb.at[h, y], Y, y, ny)
+        return scan_copy(1, h, d, tb.at[h], rb.at[h, d - 1], Y, y, ny)
 
     def b_recv(h, d):
-        return scan_copy(1, h, d, tb.at[h], rb.at[h, lax.rem(y + ny - d, ny)], Y, y, ny)
+        return scan_copy(1, h, d, tb.at[h], rb.at[h, d - 1], Y, y, ny)
 
     def c_send(h, d):
         return scan_copy(2, h, d, tc.at[h], rc.at[h, d - 1], Z, z, nz)
@@ -184,29 +194,46 @@
         tb[h] = total.astype(BF16)
         for d in far_first(ny):
             b_send(h, d).start()
-        rb[h, y] = tb[h]
-
-    def scan_c(h):
+
+        @pl.when(y == 0)
+        def _():
+            yp[h] = jnp.zeros(yp.shape[1:], F32)
+
+            @pl.when(z == 0)
+            def _():
+                scan_back(h)
+
+    def scan_low(h):
+        @pl.when(y > 0)
+        def _():
+            for d in range(1, ny):
+
+                @pl.when(y >= d)
+                def _():
+                    b_recv(h, d).wait_recv()
+                    part = rb[h, d - 1].astype(F32)
+                    yp[h] = part if d == 1 else yp[h] + part
+
+            @pl.when(z == 0)
+            def _():
+                scan_back(h)
+
+    def scan_all(h):
         for d in range(1, ny):
-            b_recv(h, d).wait_recv()
-        total = jnp.zeros(tb.shape[1:], F32)
-        before = jnp.zeros(tb.shape[1:], F32)
-        for i in range(ny):
-            part = rb[h, i].astype(F32)
-            total += part
-            before += jnp.where(i < y, part, 0.0)
+
+            @pl.when(y < d)
+            def _():
+                b_recv(h, d).wait_recv()
+
+        total = tb[h].astype(F32)
+        for d in range(1, ny):
+            total += rb[h, d - 1].astype(F32)
         tc[h] = total.astype(BF16)
         for d in far_first(nz):
 
             @pl.when(z + d < nz)
             def _():
                 c_send(h, d).start()
-
-        yp[h] = before
-
-        @pl.when(z == 0)
-        def _():
-            scan_back(h)
 
     def scan_d(h):
         @pl.when(z > 0)
@@ -247,22 +274,23 @@
 
     wk_copy.wait()
     keys(c)
+    wv_copy[0].wait()
     for h in range(heads):
         wo_copy(h).start(priority=1)
-    wv_copy[0].wait()
     values(c, 0)
-    wv_copy[1].wait()
     wq_copy.start(priority=1)
     for s in wg_copy:
         s.start(priority=1)
-    values(c, 1)
     for i in range(token_steps):
         x_recv(i).wait_recv()
     keys(other)
     values(other, 0)
+    later_are_in(0)
     scan_a((0, 1))
+    wv_copy[1].wait()
     wo_copy(0).wait()
     wo_send(0).start()
+    values(c, 1)
     values(other, 1)
     scan_a((2, 3))
 
@@ -291,6 +319,7 @@
 
     wq_copy.wait()
     queries(0)
+    later_are_in(1)
     scan_b(0)
     wo_copy(1).wait()
     wo_send(1).start()
@@ -301,30 +330,63 @@
     gates(0, 0)
     scan_b(2)
     scan_b(3)
-
-    @pl.when(z + 1 < nz)
-    def _():
-        pl.semaphore_wait(zsem, nz - 1 - z)
-
-    scan_c(0)
     wo_copy(2).wait()
     wo_send(2).start()
     gates(1, 0)
-    scan_c(1)
+    scan_low(0)
+    scan_low(1)
+    later_are_in(2)
+
+    @pl.when(y > 0)
+    def _():
+        scan_all(0)
+        scan_all(1)
+
     gates(0, 1)
-    scan_c(2)
-    scan_c(3)
-    scan_d(0)
+
+    @pl.when(y == 0)
+    def _():
+        scan_all(0)
+        scan_all(1)
+
     local(0)
+    scan_low(2)
+    scan_low(3)
+
+    @pl.when(y > 0)
+    def _():
+        scan_all(2)
+        scan_all(3)
+
+
+    @pl.when(y > 0)
+    def _():
+        scan_d(0)
+        scan_d(1)
+
     local(1)
-    scan_d(1)
+
+    @pl.when((y == 0) & (c == 0))
+    def _():
+        scan_all(2)
+        scan_all(3)
+
+    @pl.when(y == 0)
+    def _():
+        scan_d(0)
+        scan_d(1)
+
+
+    @pl.when((y == 0) & (c == 1))
+    def _():
+        scan_all(2)
+        scan_all(3)
+
     wo_copy(3).wait()
     wo_send(3).start()
     gates(1, 1)
     scan_d(2)
     scan_d(3)
-    local(2)
-    local(3)
 
     def g_send(h):
         return remote(gsnd.at[h], gall.at[h, 1], gs_s.at[h], gs_r.at[h], {TP: other})
@@ -365,14 +427,18 @@
     scan_end(1)
     carried(1)
     g_send(1).start()
-    for h in range(2, heads):
-        scan_end(h)
-        arrived(h - 2)
-        carried(h)
-        project(h - 2, first)
-        g_send(h).start()
-        project(h - 2, rest)
-    for h in range(heads - 2, heads):
+    local(2)
+    local(3)
+    scan_end(2)
+    carried(2)
+    g_send(2).start()
+    scan_end(3)
+    arrived(0)
+    carried(3)
+    project(0, first)
+    g_send(3).start()
+    project(0, rest)
+    for h in range(1, heads):
         arrived(h)
         project(h, first)
         project(h, rest)
@@ -424,7 +490,7 @@
         vmem((heads, nx, *quarter), BF16),
         vmem((heads, nx, *quarter), BF16),
         vmem((heads, *quarter), BF16),
-        vmem((heads, ny, *quarter), BF16),
+        vmem((heads, ny - 1, *quarter), BF16),
         vmem((heads, *quarter), F32),
         vmem((heads, *quarter), BF16),
         vmem((heads, nz - 1, *quarter), BF16),
@@ -447,7 +513,7 @@
         dma((heads,)),
         dma((4, heads, most)),
         dma((4, heads, most)),
-        pltpu.SemaphoreType.REGULAR,
+        pltpu.SemaphoreType.REGULAR((3,)),
     ]
     hbm = pl.BlockSpec(memory_space=pl.ANY)
     return pl.pallas_call(

time: 36.4 us -> 35.9 us (0.986)
  the two profiles are of different devices: /device:TPU:1 before, /device:TPU:32 now
where the time goes in v4:
time: 35.9 us; the launch traced here: 35.7 us
  Pallas kernels  34.4 us (96%)
  local copies, waits for them, and re-layouts  1.32 us (4%)
    pallas_call x1, Pallas kernels, on_device(): pl.pallas_call(functools.partial(mixer, sizes), out_shape=pltpu.VMEM((row...  34.4 us
    unnamed x1, local copies, waits for them, and re-layouts  1.32 us

profile of v4, /device:TPU:32, one launch (start us, length us, event | category | flops | bytes accessed | tf_op | source)
XLA Modules:
  0.0 35.7 jit_solution(8842288017152820877)
XLA Ops:
  0.0 34.4 %mixer.1 = bf16[256,4096]{1,0:T(8,128)(2,1)S(1)} custom-call(bf16[256,4096]{1,0:T(8,128)(2,1)} %tok.1, f32[1,4096]{1,0:T(1,128)} %bitcast.3, bf16[4096,512]{1,0:T(8,128)(2,1)} %wq.1, bf16[4096,512]{1,0:T(8,128)(2,1)} %wk.1, bf16[4096,1024]{1,0:T(8,128)(2,1)} %wv.1, bf16[4096,1024]{1,0:T(8,128)(2,1)} %wg.1, f32[1,512]{1,0:T(1,128)} %bitcast.5, ...), custom_call_target="tpu_custom_call" | custom-call | tf_op jit(solution)/shard_map/mixer/pallas_call | solution.py:519
  34.4 1.3 %copy.11 = bf16[256,4096]{1,0:T(8,128)(2,1)} copy(bf16[256,4096]{1,0:T(8,128)(2,1)S(1)} %mixer.1) | data formatting | bytes 4194304

commit v5 on v4

--- a/solution.py
+++ b/solution.py
@@ -33,11 +33,11 @@
 def mixer(
     sizes,
     tok, gain, wq, wk, wv, wg, bias, hgain, wo,
-    out,
-    xn, wkb, wvb, wqb, wgb, wob, gainb, biasb, hgainb,
-    kb, qb, vb, gsb, lob, acc,
+    acc, gall, wob,
+    xn, wkb, wvb, wqb, wgb, wfirst, gainb, biasb, hgainb,
+    kb, qb, vb, gsb, lob,
     sa, ra, tb, rb, yp, tc, rc, dd, pd,
-    gall, gsnd,
+    gfirst, gsnd,
     tok_sem, small_sem, k_sem, v_sem, q_sem, g_sem, wo_sem,
     xs, xr, ps, pr, gs_s, gs_r, scan_s, scan_r, line_sem,
 ):
@@ -48,7 +48,9 @@
     chunk = HEAD_K // nx
     token_steps = tok_sem.shape[0]
     step_rows = rows // token_steps
-    model = out.shape[1]
+    model = acc.shape[1]
+    wpart = lambda h, i: wob.at[h - 2, i] if h > 1 else wfirst.at[i, h]
+    gpart = lambda h, i: gall.at[h - 2, i] if h > 1 else gfirst.at[i, h]
     z, y, x, c = (lax.axis_index(a) for a in SP_TP)
     other = 1 - c
     chip = (z * ny + y) * nx + x
@@ -67,10 +69,10 @@
     wg_copy = [pltpu.make_async_copy(wg.at[:, pl.ds(p * v2, v2)], wgb.at[p], g_sem.at[p]) for p in range(pairs)]
 
     def wo_copy(h):
-        return pltpu.make_async_copy(wo.at[pl.ds(h * HEAD_V, HEAD_V), :], wob.at[h, 0], wo_sem.at[h])
+        return pltpu.make_async_copy(wo.at[pl.ds(h * HEAD_V, HEAD_V), :], wpart(h, 0), wo_sem.at[h])
 
     def wo_send(h):
-        return remote(wob.at[h, 0], wob.at[h, 1], ps.at[h], pr.at[h], {TP: other})
+        return remote(wpart(h, 0), wpart(h, 1), ps.at[h], pr.at[h], {TP: other})
 
     for s in small:
         s.start()
@@ -389,59 +391,48 @@
     scan_d(3)
 
     def g_send(h):
-        return remote(gsnd.at[h], gall.at[h, 1], gs_s.at[h], gs_r.at[h], {TP: other})
-
-    def carried(h):
-        start = pd[h].reshape(HEAD_K, HEAD_V)
+        return remote(gsnd.at[h], gpart(h, 1), gs_s.at[h], gs_r.at[h], {TP: other})
+
+    def carried(pair):
         for own in (False, True):
-            b = c if own else other
-            o = lob[b, h].astype(F32) + dot(qb[b, h], start)
-            scale = lax.rsqrt(jnp.mean(o * o, axis=-1, keepdims=True) + EPS)
-            gated = (o * scale * gsb[b, h].astype(F32)).astype(BF16)
-            if own:
-                gall[h, 0] = gated
-            else:
-                gsnd[h] = gated
-
-    def project(h, steps):
-        gated = jnp.concatenate([gall[h, 0], gall[h, 1]], axis=1)
-        for n in steps:
+            for h in pair:
+                b = c if own else other
+                start = pd[h].reshape(HEAD_K, HEAD_V)
+                o = lob[b, h].astype(F32) + dot(qb[b, h], start)
+                scale = lax.rsqrt(jnp.mean(o * o, axis=-1, keepdims=True) + EPS)
+                gated = (o * scale * gsb[b, h].astype(F32)).astype(BF16)
+                if own:
+                    gpart(h, 0)[...] = gated
+                else:
+                    gsnd[h] = gated
+        for h in pair:
+            g_send(h).start()
+
+    def project(i):
+        gated = jnp.concatenate([gfirst[i, 0], gfirst[i, 1]], axis=1)
+        for n in range(model // UNIT):
             at = slice(n * UNIT, (n + 1) * UNIT)
-            part = dot(gated, wob[h, :, :, at].reshape(2 * HEAD_V, UNIT))
-            if h:
-                part += acc[n]
-            if h < heads - 1:
-                acc[n] = part
-            else:
-                out[:, at] = part.astype(BF16)
-
-    first, rest = range(0, model // UNIT // 2), range(model // UNIT // 2, model // UNIT)
+            part = dot(gated, wfirst[i, :, :, at].reshape(2 * HEAD_V, UNIT))
+            acc[:, at] = acc[:, at] + part if i else part
 
     def arrived(h):
         g_send(h).wait_recv()
         wo_send(h).wait_recv()
 
-    scan_end(0)
-    carried(0)
-    g_send(0).start()
-    scan_end(1)
-    carried(1)
-    g_send(1).start()
     local(2)
     local(3)
+    scan_end(0)
+    scan_end(1)
+    carried((0, 1))
+    project(0)
     scan_end(2)
-    carried(2)
-    g_send(2).start()
     scan_end(3)
+    carried((2, 3))
     arrived(0)
-    carried(3)
-    project(0, first)
-    g_send(3).start()
-    project(0, rest)
-    for h in range(1, heads):
+    arrived(1)
+    project(1)
+    for h in range(2, heads):
         arrived(h)
-        project(h, first)
-        project(h, rest)
 
     for i in range(token_steps):
         x_send(i).wait_send()
@@ -458,6 +449,21 @@
             @pl.when(z + d < nz)
             def _():
                 c_send(h, d).wait_send()
+
+
+def finish(acc, gated, weight, out, stage, sem):
+    rows, model = acc.shape
+    depth = weight.shape[0] * 2 * HEAD_V
+    left = jnp.concatenate([gated[h, i] for h in range(weight.shape[0]) for i in range(2)], axis=1)
+    copies = []
+    for n in range(model // UNIT):
+        at = slice(n * UNIT, (n + 1) * UNIT)
+        right = weight[:, :, :, at].reshape(depth, UNIT)
+        stage[n] = (acc[:, at] + dot(left, right)).astype(BF16)
+        copies.append(pltpu.make_async_copy(stage.at[n], out.at[:, pl.ds(n * UNIT, UNIT)], sem.at[n]))
+        copies[-1].start()
+    for copy in copies:
+        copy.wait()
 
 
 def on_device(sizes, tok, gain, wq, wk, wv, wg, bias, hgain, wo):
@@ -477,7 +483,7 @@
         vmem((pairs, width, 2 * HEAD_V), BF16),
         vmem((width, key_width), BF16),
         vmem((pairs, width, 2 * HEAD_V), BF16),
-        vmem((heads, 2, HEAD_V, model), BF16),
+        vmem((2, 2, HEAD_V, model), BF16),
         vmem((1, width), F32),
         vmem((1, key_width), F32),
         vmem((1, value_width), F32),
@@ -486,7 +492,6 @@
         vmem((2, heads, rows, HEAD_V), BF16),
         vmem((2, heads, rows, HEAD_V), BF16),
         vmem((2, heads, rows, HEAD_V), BF16),
-        vmem((model // UNIT, rows, UNIT), F32),
         vmem((heads, nx, *quarter), BF16),
         vmem((heads, nx, *quarter), BF16),
         vmem((heads, *quarter), BF16),
@@ -496,7 +501,7 @@
         vmem((heads, nz - 1, *quarter), BF16),
         vmem((heads, nx, *quarter), BF16),
         vmem((heads, nx, *quarter), BF16),
-        vmem((heads, 2, rows, HEAD_V), BF16),
+        vmem((2, 2, rows, HEAD_V), BF16),
         vmem((heads, rows, HEAD_V), BF16),
         dma((token_steps,)),
         dma((3,)),
@@ -516,19 +521,33 @@
         pltpu.SemaphoreType.REGULAR((3,)),
     ]
     hbm = pl.BlockSpec(memory_space=pl.ANY)
-    return pl.pallas_call(
+    in_vmem = pl.BlockSpec(memory_space=vmem)
+    parts = pl.pallas_call(
         functools.partial(mixer, sizes),
-        out_shape=pltpu.VMEM((rows, model), BF16),
+        out_shape=(
+            vmem((rows, model), F32),
+            vmem((heads - 2, 2, rows, HEAD_V), BF16),
+            vmem((heads - 2, 2, HEAD_V, model), BF16),
+        ),
         in_specs=[hbm] * 9,
-        out_specs=pl.BlockSpec(memory_space=pltpu.VMEM),
+        out_specs=[in_vmem] * 3,
         scratch_shapes=scratch,
         compiler_params=pltpu.CompilerParams(
-            collective_id=0, has_side_effects=True, vmem_limit_bytes=64_500_000
+            collective_id=0, has_side_effects=True, vmem_limit_bytes=52_500_000
         ),
         name="mixer",
     )(
         tok, gain.reshape(1, -1), wq, wk, wv, wg, bias.reshape(1, -1), hgain.reshape(1, -1), wo
     )
+    return pl.pallas_call(
+        finish,
+        out_shape=jax.ShapeDtypeStruct((rows, model), BF16),
+        in_specs=[in_vmem] * 3,
+        out_specs=hbm,
+        scratch_shapes=[vmem((model // UNIT, rows, UNIT), BF16), dma((model // UNIT,))],
+        compiler_params=pltpu.CompilerParams(vmem_limit_bytes=8_000_000),
+        name="finish",
+    )(*parts)
 
 
 def solution(mesh, sizes=(4, 4, 4)):

time: 35.9 us -> 34.3 us (0.955)
  local copies, waits for them, and re-layouts: 1.32 us -> 0 us
  Pallas kernels: 34.4 us -> 33.6 us
    unnamed x1 -> x0, local copies, waits for them, and re-layouts: 1.32 us -> none
    pallas_call x1 -> x2, Pallas kernels: 34.4 us -> 33.6 us  [the longest x1 30.5 us: on_device(): pl.pallas_call(functools.partial(mixer, sizes), out_shape=(vmem((rows, mo...]
where the time goes in v5:
time: 34.3 us; the launch traced here: 33.8 us
  Pallas kernels  33.6 us (98%)
    pallas_call x1, Pallas kernels, on_device(): pl.pallas_call(functools.partial(mixer, sizes), out_shape=(vmem((rows, mo...  30.5 us
    pallas_call x1, Pallas kernels, on_device(): pl.pallas_call(finish, out_shape=jax.ShapeDtypeStruct((rows, model), BF16...  3.11 us

profile of v5, /device:TPU:32, one launch (start us, length us, event | category | flops | bytes accessed | tf_op | source)
XLA Modules:
  0.0 33.8 jit_solution(12365749308751731739)
XLA Ops:
  0.0 30.5 %mixer.1 = (f32[256,4096]{1,0:T(8,128)S(1)}, bf16[2,2,256,256]{3,2,1,0:T(8,128)(2,1)S(1)}, bf16[2,2,256,4096]{3,2,1,0:T(8,128)(2,1)S(1)}) custom-call(bf16[256,4096]{1,0:T(8,128)(2,1)} %tok.1, f32[1,4096]{1,0:T(1,128)} %bitcast.3, bf16[4096,512]{1,0:T(8,128)(2,1)} %wq.1, bf16[4096,512]{1,0:T(8,128)(2,1)} %wk.1, bf16[4096,1024]{1,0:T(8,128)(2,1)} %wv.1, ...), custom_call_target="tpu_custom_call" | custom-call | tf_op jit(solution)/shard_map/mixer/pallas_call | solution.py:525
  30.5 3.1 %finish.1 = bf16[256,4096]{1,0:T(8,128)(2,1)} custom-call(f32[256,4096]{1,0:T(8,128)S(1)} %get-tuple-element.8.acc, bf16[2,2,256,256]{3,2,1,0:T(8,128)(2,1)S(1)} %get-tuple-element.9.gated, bf16[2,2,256,4096]{3,2,1,0:T(8,128)(2,1)S(1)} %get-tuple-element.10.weight), custom_call_target="tpu_custom_call" | custom-call | tf_op jit(solution)/shard_map/finish/pallas_call | solution.py:542

commit v6 on v5

--- a/solution.py
+++ b/solution.py
@@ -49,8 +49,14 @@
     token_steps = tok_sem.shape[0]
     step_rows = rows // token_steps
     model = acc.shape[1]
-    wpart = lambda h, i: wob.at[h - 2, i] if h > 1 else wfirst.at[i, h]
-    gpart = lambda h, i: gall.at[h - 2, i] if h > 1 else gfirst.at[i, h]
+
+    def part_of(first, last, h, i):
+        if i and h > 1:
+            return last.at[h - 2]
+        return first.at[2 if i else h // 2, h % 2]
+
+    wpart = functools.partial(part_of, wfirst, wob)
+    gpart = functools.partial(part_of, gfirst, gall)
     z, y, x, c = (lax.axis_index(a) for a in SP_TP)
     other = 1 - c
     chip = (z * ny + y) * nx + x
@@ -408,12 +414,13 @@
         for h in pair:
             g_send(h).start()
 
-    def project(i):
-        gated = jnp.concatenate([gfirst[i, 0], gfirst[i, 1]], axis=1)
+    def project(groups):
+        lo, hi = groups[0], groups[-1] + 1
+        gated = jnp.concatenate([gfirst[g, h] for g in groups for h in range(2)], axis=1)
         for n in range(model // UNIT):
             at = slice(n * UNIT, (n + 1) * UNIT)
-            part = dot(gated, wfirst[i, :, :, at].reshape(2 * HEAD_V, UNIT))
-            acc[:, at] = acc[:, at] + part if i else part
+            part = dot(gated, wfirst[lo:hi, :, :, at].reshape((hi - lo) * 2 * HEAD_V, UNIT))
+            acc[:, at] = acc[:, at] + part if lo else part
 
     def arrived(h):
         g_send(h).wait_recv()
@@ -424,13 +431,26 @@
     scan_end(0)
     scan_end(1)
     carried((0, 1))
-    project(0)
+    project((0,))
     scan_end(2)
     scan_end(3)
     carried((2, 3))
+
+    @pl.when(c == 1)
+    def _():
+        project((1,))
+
     arrived(0)
     arrived(1)
-    project(1)
+
+    @pl.when(c == 1)
+    def _():
+        project((2,))
+
+    @pl.when(c == 0)
+    def _():
+        project((1, 2))
+
     for h in range(2, heads):
         arrived(h)
 
@@ -453,12 +473,11 @@
 
 def finish(acc, gated, weight, out, stage, sem):
     rows, model = acc.shape
-    depth = weight.shape[0] * 2 * HEAD_V
-    left = jnp.concatenate([gated[h, i] for h in range(weight.shape[0]) for i in range(2)], axis=1)
+    left = jnp.concatenate([gated[0], gated[1]], axis=1)
     copies = []
     for n in range(model // UNIT):
         at = slice(n * UNIT, (n + 1) * UNIT)
-        right = weight[:, :, :, at].reshape(depth, UNIT)
+        right = weight[:, :, at].reshape(2 * HEAD_V, UNIT)
         stage[n] = (acc[:, at] + dot(left, right)).astype(BF16)
         copies.append(pltpu.make_async_copy(stage.at[n], out.at[:, pl.ds(n * UNIT, UNIT)], sem.at[n]))
         copies[-1].start()
@@ -483,7 +502,7 @@
         vmem((pairs, width, 2 * HEAD_V), BF16),
         vmem((width, key_width), BF16),
         vmem((pairs, width, 2 * HEAD_V), BF16),
-        vmem((2, 2, HEAD_V, model), BF16),
+        vmem((3, 2, HEAD_V, model), BF16),
         vmem((1, width), F32),
         vmem((1, key_width), F32),
         vmem((1, value_width), F32),
@@ -501,7 +520,7 @@
         vmem((heads, nz - 1, *quarter), BF16),
         vmem((heads, nx, *quarter), BF16),
         vmem((heads, nx, *quarter), BF16),
-        vmem((2, 2, rows, HEAD_V), BF16),
+        vmem((3, 2, rows, HEAD_V), BF16),
         vmem((heads, rows, HEAD_V), BF16),
         dma((token_steps,)),
         dma((3,)),
@@ -526,14 +545,14 @@
         functools.partial(mixer, sizes),
         out_shape=(
             vmem((rows, model), F32),
-            vmem((heads - 2, 2, rows, HEAD_V), BF16),
-            vmem((heads - 2, 2, HEAD_V, model), BF16),
+            vmem((2, rows, HEAD_V), BF16),
+            vmem((2, HEAD_V, model), BF16),
         ),
         in_specs=[hbm] * 9,
         out_specs=[in_vmem] * 3,
         scratch_shapes=scratch,
         compiler_params=pltpu.CompilerParams(
-            collective_id=0, has_side_effects=True, vmem_limit_bytes=52_500_000
+            collective_id=0, has_side_effects=True, vmem_limit_bytes=57_000_000
         ),
         name="mixer",
     )(

time: 34.3 us -> 34.7 us (1.012); the launches traced: 33.8 us -> 34.6 us
  Pallas kernels: 33.6 us -> 34.4 us
    pallas_call x1, Pallas kernels: 30.5 us -> 32.4 us  [on_device(): pl.pallas_call(functools.partial(mixer, sizes), out_shape=(vmem((rows, mo...]
    pallas_call x1, Pallas kernels: 3.11 us -> 2.04 us  [on_device(): pl.pallas_call(finish, out_shape=jax.ShapeDtypeStruct((rows, model), BF16...]
where the time goes in v6:
time: 34.7 us; the launch traced here: 34.6 us
  Pallas kernels  34.4 us (99%)
    pallas_call x1, Pallas kernels, on_device(): pl.pallas_call(functools.partial(mixer, sizes), out_shape=(vmem((rows, mo...  32.4 us
    pallas_call x1, Pallas kernels, on_device(): pl.pallas_call(finish, out_shape=jax.ShapeDtypeStruct((rows, model), BF16...  2.04 us

profile of v6, /device:TPU:32, one launch (start us, length us, event | category | flops | bytes accessed | tf_op | source)
XLA Modules:
  0.0 34.6 jit_solution(10874659879461713774)
XLA Ops:
  0.0 32.4 %mixer.1 = (f32[256,4096]{1,0:T(8,128)S(1)}, bf16[2,256,256]{2,1,0:T(8,128)(2,1)S(1)}, bf16[2,256,4096]{2,1,0:T(8,128)(2,1)S(1)}) custom-call(bf16[256,4096]{1,0:T(8,128)(2,1)} %tok.1, f32[1,4096]{1,0:T(1,128)} %bitcast.3, bf16[4096,512]{1,0:T(8,128)(2,1)} %wq.1, bf16[4096,512]{1,0:T(8,128)(2,1)} %wk.1, bf16[4096,1024]{1,0:T(8,128)(2,1)} %wv.1, ...), custom_call_target="tpu_custom_call" | custom-call | tf_op jit(solution)/shard_map/mixer/pallas_call | solution.py:544
  32.4 2.0 %finish.1 = bf16[256,4096]{1,0:T(8,128)(2,1)} custom-call(f32[256,4096]{1,0:T(8,128)S(1)} %get-tuple-element.8.acc, bf16[2,256,256]{2,1,0:T(8,128)(2,1)S(1)} %get-tuple-element.9.gated, bf16[2,256,4096]{2,1,0:T(8,128)(2,1)S(1)} %get-tuple-element.10.weight), custom_call_target="tpu_custom_call" | custom-call | tf_op jit(solution)/shard_map/finish/pallas_call | solution.py:561

commit v7 on v5

--- a/solution.py
+++ b/solution.py
@@ -63,8 +63,20 @@
     small = [(gain, gainb), (bias, biasb), (hgain, hgainb)]
     small = [pltpu.make_async_copy(a, b, small_sem.at[i]) for i, (a, b) in enumerate(small)]
     v2 = 2 * HEAD_V
-    wk_copy = pltpu.make_async_copy(wk, wkb, k_sem.at[0])
-    wv_copy = [pltpu.make_async_copy(wv.at[:, pl.ds(p * v2, v2)], wvb.at[p], v_sem.at[p]) for p in range(pairs)]
+    step = width // k_sem.shape[0]
+    wk_copy = [
+        pltpu.make_async_copy(wk.at[pl.ds(i * step, step), :], wkb.at[pl.ds(i * step, step), :], k_sem.at[i])
+        for i in range(k_sem.shape[0])
+    ]
+    wv_copy = [
+        [
+            pltpu.make_async_copy(
+                wv.at[pl.ds(i * step, step), pl.ds(p * v2, v2)], wvb.at[p, pl.ds(i * step, step), :], v_sem.at[p, i]
+            )
+            for i in range(k_sem.shape[0])
+        ]
+        for p in range(pairs)
+    ]
     wq_copy = pltpu.make_async_copy(wq, wqb, q_sem.at[0])
     wg_copy = [pltpu.make_async_copy(wg.at[:, pl.ds(p * v2, v2)], wgb.at[p], g_sem.at[p]) for p in range(pairs)]
 
@@ -78,7 +90,8 @@
         s.start()
     for i in range(token_steps):
         token_copy(i).start()
-    wk_copy.start(priority=1)
+    for s in wk_copy:
+        s.start(priority=1)
 
     barrier = pltpu.get_barrier_semaphore()
     lines = [(X, x, nx), (Y, y, ny), (Z, z, nz)]
@@ -119,9 +132,11 @@
     for i in range(token_steps):
         token_copy(i).wait()
         if i == 0:
-            wv_copy[0].start(priority=1)
+            for s in wv_copy[0]:
+                s.start(priority=1)
         if i == token_steps - 1:
-            wv_copy[1].start(priority=1)
+            for s in wv_copy[1]:
+                s.start(priority=1)
 
         for g in range(step_rows // 16):
             r = pl.ds(i * step_rows + g * 16, 16)
@@ -274,9 +289,11 @@
         for i in range(2):
             vb[b, 2 * p + i] = v[:, i * HEAD_V : (i + 1) * HEAD_V]
 
-    wk_copy.wait()
+    for s in wk_copy:
+        s.wait()
     keys(c)
-    wv_copy[0].wait()
+    for s in wv_copy[0]:
+        s.wait()
     for h in range(heads):
         wo_copy(h).start(priority=1)
     values(c, 0)
@@ -289,7 +306,8 @@
     values(other, 0)
     later_are_in(0)
     scan_a((0, 1))
-    wv_copy[1].wait()
+    for s in wv_copy[1]:
+        s.wait()
     wo_copy(0).wait()
     wo_send(0).start()
     values(c, 1)
@@ -461,7 +479,9 @@
         right = weight[:, :, :, at].reshape(depth, UNIT)
         stage[n] = (acc[:, at] + dot(left, right)).astype(BF16)
         copies.append(pltpu.make_async_copy(stage.at[n], out.at[:, pl.ds(n * UNIT, UNIT)], sem.at[n]))
-        copies[-1].start()
+        if n:
+            copies[n - 1].start()
+    copies[-1].start()
     for copy in copies:
         copy.wait()
 
@@ -505,8 +525,8 @@
         vmem((heads, rows, HEAD_V), BF16),
         dma((token_steps,)),
         dma((3,)),
-        dma((1,)),
-        dma((pairs,)),
+        dma((4,)),
+        dma((pairs, 4)),
         dma((1,)),
         dma((pairs,)),
         dma((heads,)),

time: 34.3 us -> 34.3 us (level)
  no operation moved by 1% of the time
where the time goes in v7:
time: 34.3 us; the launch traced here: 33.8 us
  Pallas kernels  33.7 us (98%)
    pallas_call x1, Pallas kernels, on_device(): pl.pallas_call(functools.partial(mixer, sizes), out_shape=(vmem((rows, mo...  30.5 us
    pallas_call x1, Pallas kernels, on_device(): pl.pallas_call(finish, out_shape=jax.ShapeDtypeStruct((rows, model), BF16...  3.2 us

profile of v7, /device:TPU:32, one launch (start us, length us, event | category | flops | bytes accessed | tf_op | source)
XLA Modules:
  0.0 33.8 jit_solution(17255530408104907406)
XLA Ops:
  0.0 30.5 %mixer.1 = (f32[256,4096]{1,0:T(8,128)S(1)}, bf16[2,2,256,256]{3,2,1,0:T(8,128)(2,1)S(1)}, bf16[2,2,256,4096]{3,2,1,0:T(8,128)(2,1)S(1)}) custom-call(bf16[256,4096]{1,0:T(8,128)(2,1)} %tok.1, f32[1,4096]{1,0:T(1,128)} %bitcast.3, bf16[4096,512]{1,0:T(8,128)(2,1)} %wq.1, bf16[4096,512]{1,0:T(8,128)(2,1)} %wk.1, bf16[4096,1024]{1,0:T(8,128)(2,1)} %wv.1, ...), custom_call_target="tpu_custom_call" | custom-call | tf_op jit(solution)/shard_map/mixer/pallas_call | solution.py:545
  30.5 3.2 %finish.1 = bf16[256,4096]{1,0:T(8,128)(2,1)} custom-call(f32[256,4096]{1,0:T(8,128)S(1)} %get-tuple-element.8.acc, bf16[2,2,256,256]{3,2,1,0:T(8,128)(2,1)S(1)} %get-tuple-element.9.gated, bf16[2,2,256,4096]{3,2,1,0:T(8,128)(2,1)S(1)} %get-tuple-element.10.weight), custom_call_target="tpu_custom_call" | custom-call | tf_op jit(solution)/shard_map/finish/pallas_call | solution.py:562

commit v8 on v5

--- a/solution.py
+++ b/solution.py
@@ -461,7 +461,9 @@
         right = weight[:, :, :, at].reshape(depth, UNIT)
         stage[n] = (acc[:, at] + dot(left, right)).astype(BF16)
         copies.append(pltpu.make_async_copy(stage.at[n], out.at[:, pl.ds(n * UNIT, UNIT)], sem.at[n]))
-        copies[-1].start()
+        if n:
+            copies[n - 1].start()
+    copies[-1].start()
     for copy in copies:
         copy.wait()
 

time: 34.3 us -> 34.4 us (level)
  no operation moved by 1% of the time
where the time goes in v8:
time: 34.4 us; the launch traced here: 33.8 us
  Pallas kernels  33.7 us (98%)
    pallas_call x1, Pallas kernels, on_device(): pl.pallas_call(functools.partial(mixer, sizes), out_shape=(vmem((rows, mo...  30.5 us
    pallas_call x1, Pallas kernels, on_device(): pl.pallas_call(finish, out_shape=jax.ShapeDtypeStruct((rows, model), BF16...  3.2 us

profile of v8, /device:TPU:32, one launch (start us, length us, event | category | flops | bytes accessed | tf_op | source)
XLA Modules:
  0.0 33.8 jit_solution(387878687960618435)
XLA Ops:
  0.0 30.5 %mixer.1 = (f32[256,4096]{1,0:T(8,128)S(1)}, bf16[2,2,256,256]{3,2,1,0:T(8,128)(2,1)S(1)}, bf16[2,2,256,4096]{3,2,1,0:T(8,128)(2,1)S(1)}) custom-call(bf16[256,4096]{1,0:T(8,128)(2,1)} %tok.1, f32[1,4096]{1,0:T(1,128)} %bitcast.3, bf16[4096,512]{1,0:T(8,128)(2,1)} %wq.1, bf16[4096,512]{1,0:T(8,128)(2,1)} %wk.1, bf16[4096,1024]{1,0:T(8,128)(2,1)} %wv.1, ...), custom_call_target="tpu_custom_call" | custom-call | tf_op jit(solution)/shard_map/mixer/pallas_call | solution.py:527
  30.5 3.2 %finish.1 = bf16[256,4096]{1,0:T(8,128)(2,1)} custom-call(f32[256,4096]{1,0:T(8,128)S(1)} %get-tuple-element.8.acc, bf16[2,2,256,256]{3,2,1,0:T(8,128)(2,1)S(1)} %get-tuple-element.9.gated, bf16[2,2,256,4096]{3,2,1,0:T(8,128)(2,1)S(1)} %get-tuple-element.10.weight), custom_call_target="tpu_custom_call" | custom-call | tf_op jit(solution)/shard_map/finish/pallas_call | solution.py:544
